TPU v7x, 128 devices: a whole 4x4x4 slice. The times are simulated.
128 devices in a mesh: sp: 32 (over z, y, core), tp: 4 (over x).
Axes of the slice: x: 4, y: 4, z: 4, core: 2. Of those that a mesh axis runs over, the one named last changes fastest.
Arguments:
- queries: bfloat16 [12288, 2048], P('sp', 'tp'), may hold values from -6 to 6
- keys: bfloat16 [12288, 2048], P('sp', 'tp'), may hold values from -6 to 6
- values: bfloat16 [12288, 2048], P('sp', 'tp'), may hold values from -6 to 6
- gates: bfloat16 [12288, 2048], P('sp', 'tp'), may hold values from -8 to 8
- decay_pre: float32 [32, 12288], P('tp', 'sp'), may hold values from -18 to 3
- beta_pre: float32 [32, 12288], P('tp', 'sp'), may hold values from -10 to 3
- out_gain: float32 [64], replicated, may hold values from 0.1 to 1.9
- w_out: bfloat16 [2048, 2048], P('tp'), may hold values from -0.125 to 0.125
- stream: bfloat16 [12288, 2048], P(('sp', 'tp')), may hold values from -6 to 6
- norm_gain: float32 [2048], replicated, may hold values from 0.1 to 1.9
- w_gate: bfloat16 [2048, 5632], P('sp', 'tp'), may hold values from -0.125 to 0.125
- w_up: bfloat16 [2048, 5632], P('sp', 'tp'), may hold values from -0.125 to 0.125
- w_down: bfloat16 [5632, 2048], P('tp', 'sp'), may hold values from -0.078125 to 0.078125
Outputs:
- updated: bfloat16 [12288, 2048], P(('sp', 'tp'))
All inputs are finite; a program needn't handle non-finite values.
Results may differ from a plain program's by a relative error of at most 0.019.
Values may be sent and summed in bfloat16 or wider, within the bound.
No kernel may reach another device: no remote copies, remote signals or barrier semaphores. Data moves between devices by JAX's collectives and lax.ppermute only.
A program may use at most 128 MiB of HBM per device.

v0:
```python
import functools

import jax
import jax.numpy as jnp
from jax import lax
from jax.experimental import pallas as pl
from jax.experimental.pallas import tpu as pltpu
from jax.sharding import Mesh
from jax.sharding import PartitionSpec as P


HEAD_DIM = 64
PAIR = 2 * HEAD_DIM
CHUNK = 128
SP = ("sp_0", "sp_1", "sp_2")
SP_TP = ("sp_0", "sp_1", "sp_2", "tp")
EPSILON = 1e-06
BF = jnp.bfloat16
F32 = jnp.float32
NT = (((1,), (1,)), ((), ()))


FULL = pl.BlockSpec(memory_space=pltpu.VMEM)
FAR = pl.BlockSpec(memory_space=pl.ANY)


def call(kernel, arrays, shapes, scratch=(), far=(), mib=16):
    near = [pltpu.with_memory_space_constraint(x, pltpu.VMEM) for x in arrays]
    return pl.pallas_call(
        kernel,
        in_specs=[FAR] * len(far) + [FULL] * len(near),
        out_specs=[FULL] * len(shapes),
        out_shape=[pltpu.VMEM(shape, dtype) for shape, dtype in shapes],
        scratch_shapes=scratch,
        compiler_params=pltpu.CompilerParams(vmem_limit_bytes=mib << 20),
    )(*far, *near)


def ring(size, k):
    return [(i, (i + k) % size) for i in range(size)]


def dot(a, b):
    return jnp.dot(a, b, preferred_element_type=F32)


def dot_nt(a, b):
    return lax.dot_general(a, b, NT, preferred_element_type=F32)


def silu(x):
    return x / (1.0 + jnp.exp(-x))


def places():
    row = lax.broadcasted_iota(jnp.int32, (PAIR, PAIR), 0)
    col = lax.broadcasted_iota(jnp.int32, (PAIR, PAIR), 1)
    return row, col


def half_sums(squares, ones):
    high = squares.astype(BF)
    low = (squares - high.astype(F32)).astype(BF)
    return dot(high, ones) + dot(low, ones)


def softplus(x):
    small = jnp.exp(-jnp.abs(x))
    series = small * (1.0 - small * (0.5 - small * (1.0 / 3.0 - 0.25 * small)))
    return jnp.maximum(x, 0.0) + jnp.where(small < 0.015, series, jnp.log(1.0 + small))


def turned(z):
    return pltpu.roll(z, HEAD_DIM, 1)


def split_three(x):
    high = x.astype(BF)
    rest = x - high.astype(F32)
    middle = rest.astype(BF)
    return jnp.concatenate([high, middle], axis=1), (rest - middle.astype(F32)).astype(BF)


def side_by_side(pair):
    zero = jnp.zeros_like(pair[0])
    upper = jnp.concatenate([pair[0], zero], axis=1)
    lower = jnp.concatenate([zero, pair[1]], axis=1)
    return jnp.concatenate([upper, lower], axis=0)


def halves(x):
    return x[:, :CHUNK], x[:, CHUNK:]


def keys_kernel(
    k_far_ref, v_far_ref, beta_far_ref, decay_far_ref,
    before_ref, total_ref, y_ref, d_ref, ec_ref,
    l_ref, x_ref, r_ref, f_ref, k_ref, v_ref, beta_ref, decay_ref, sems,
):
    length, width = k_ref.shape
    rate_copies = [
        pltpu.make_async_copy(decay_far_ref, decay_ref, sems.at[0]),
        pltpu.make_async_copy(beta_far_ref, beta_ref, sems.at[1]),
    ]
    row_copies = []
    for c in range(length // CHUNK):
        rows = pl.ds(c * CHUNK, CHUNK)
        for k, (far_ref, ref) in enumerate(((k_far_ref, k_ref), (v_far_ref, v_ref))):
            sem = sems.at[2 + 2 * c + k]
            row_copies.append(pltpu.make_async_copy(far_ref.at[rows], ref.at[rows], sem))
    for copy in rate_copies + row_copies:
        copy.start()
    row, col = places()
    left = col < HEAD_DIM
    top = row < HEAD_DIM
    same = left == top
    ones = jnp.where(same, 1.0, 0.0).astype(BF)
    inclusive = row >= col
    strict = row > col
    differ = row ^ col
    eye = jnp.where(row == col, 1.0, 0.0)
    off_eye = differ == HEAD_DIM
    pairs = width // PAIR
    heads = 2 * pairs
    steps = length // CHUNK

    def stacked(x):
        return jnp.concatenate([x[:, c * CHUNK : (c + 1) * CHUNK] for c in range(steps)], axis=0)

    for copy in rate_copies + row_copies:
        copy.wait()
    rates = split_three(stacked(-softplus(decay_ref[...])))
    strength = split_three(stacked(1.0 / (1.0 + jnp.exp(-beta_ref[...]))))
    triangle = jnp.where(inclusive, 1.0, 0.0).astype(BF)
    eye_bf = eye.astype(BF)
    triangle_two = jnp.concatenate([triangle, triangle], axis=1)
    cum_row = dot_nt(rates[0], triangle_two) + dot_nt(rates[1], triangle)
    cum_col = dot_nt(triangle_two, rates[0]) + dot_nt(triangle, rates[1])
    beta_col = dot_nt(jnp.concatenate([eye_bf, eye_bf], axis=1), strength[0])
    beta_col = beta_col + dot_nt(eye_bf, strength[1])

    ends = []
    for c in range(steps):
        rows = slice(c * CHUNK, (c + 1) * CHUNK)
        for p in range(pairs):
            lanes = slice(p * PAIR, (p + 1) * PAIR)
            item = c * pairs + p
            key = silu(k_ref[rows, lanes].astype(F32))
            key = (key * lax.rsqrt(half_sums(key * key, ones) + EPSILON)).astype(BF)
            y_ref[item, :, 2 * PAIR :] = key
            key_f = key.astype(F32)
            first = c * heads + 2 * p
            cums = [cum_col[:, h : h + 1] for h in (first, first + 1)]
            betas = [beta_col[:, h : h + 1] for h in (first, first + 1)]
            cum = jnp.where(left, cums[0], cums[1])
            beta = jnp.where(left, betas[0], betas[1])
            grown = jnp.exp(cum)
            ec_ref[rows, lanes] = grown
            strong = turned(key_f * (beta * grown))
            value = silu(v_ref[rows, lanes].astype(F32)) * beta
            r_ref[item, :, :CHUNK] = jnp.where(left, value, strong).astype(BF)
            r_ref[item, :, CHUNK:] = jnp.where(left, strong, value).astype(BF)
            fade = jnp.exp(cum[CHUNK - 1 : CHUNK, :] - cum)
            f_ref[item] = (key_f * fade).T.astype(BF)
            last = [jnp.exp(x[CHUNK - 1 : CHUNK, :]) for x in cums]
            ends.append(jnp.where(off_eye, jnp.where(top, last[0], last[1]), 0.0))
            owns = [jnp.where(left, key_f, 0.0), jnp.where(left, 0.0, key_f)]
            inner = dot_nt(key, jnp.concatenate(owns, axis=0).astype(BF))
            for s in range(2):
                part = slice(s * CHUNK, (s + 1) * CHUNK)
                gap = cums[s] - cum_row[first + s : first + s + 1, :]
                decay = jnp.where(inclusive, jnp.exp(gap), 0.0)
                d_ref[item, :, part] = decay.astype(BF)
                lower = jnp.where(strict, inner[:, part] * decay * betas[s], 0.0)
                l_ref[item, :, part] = lower.astype(BF)
                x_ref[item, :, part] = (eye - jnp.where(differ == 1, lower, 0.0)).astype(BF)

    items = steps * pairs

    for power in range(1, 7):
        mask = jnp.where((differ >> power) == 1, 1.0, 0.0).astype(BF)
        parts = []
        for i in range(items):
            block = side_by_side([part * mask for part in halves(l_ref[i])])
            parts.append(dot(x_ref[i], block).astype(BF))
        for i in range(items):
            x = x_ref[i]
            x_ref[i] = x - dot(parts[i], side_by_side(halves(x))).astype(BF)

    runs = [None] * pairs
    for c in range(steps):
        for p in range(pairs):
            item = c * pairs + p
            y = dot(x_ref[item], side_by_side(halves(r_ref[item]))).astype(BF)
            y_ref[item, :, : 2 * PAIR] = y
            z = jnp.where(top, *halves(dot(f_ref[item], y)))
            z = jnp.where(same, z, ends[item] - z)
            if c == 0:
                before_ref[item] = jnp.where(off_eye, 1.0, 0.0).astype(BF)
                runs[p] = z.astype(BF)
            else:
                before_ref[item] = runs[p]
                step = jnp.where(same, turned(z), 0.0).astype(BF)
                runs[p] = (dot(step, runs[p]) + jnp.where(same, z, 0.0)).astype(BF)
    for p in range(pairs):
        total_ref[p] = runs[p]


def keys_side(keys, values, beta_pre, decay_pre):
    length, width = keys.shape
    pairs = width // PAIR
    steps = length // CHUNK
    items = steps * pairs
    wide = pltpu.VMEM((items, CHUNK, 2 * CHUNK), BF)
    return call(
        keys_kernel,
        [],
        [
            ((items, PAIR, PAIR), BF),
            ((pairs, PAIR, PAIR), BF),
            ((items, CHUNK, 3 * PAIR), BF),
            ((items, CHUNK, 2 * CHUNK), BF),
            ((length, width), F32),
        ],
        [
            wide,
            wide,
            wide,
            pltpu.VMEM((items, PAIR, CHUNK), BF),
            pltpu.VMEM((length, width), BF),
            pltpu.VMEM((length, width), BF),
            pltpu.VMEM(beta_pre.shape, F32),
            pltpu.VMEM(beta_pre.shape, F32),
            pltpu.SemaphoreType.DMA((2 + 2 * steps,)),
        ],
        far=[
            pltpu.with_memory_space_constraint(x, pltpu.HBM)
            for x in (keys, values, beta_pre, decay_pre)
        ],
    )


def gates_kernel(gates_ref, gain_ref, gate_ref):
    gain = jnp.concatenate([gain_ref[...], gain_ref[...]], axis=1)
    for p in range(gates_ref.shape[1] // PAIR):
        lanes = slice(p * PAIR, (p + 1) * PAIR)
        gate_ref[:, lanes] = silu(gates_ref[:, lanes].astype(F32)) * gain


def queries_kernel(first, after_ref, q_ref, d_ref, y_ref, before_ref, ec_ref, o_ref, q1_ref):
    row, col = places()
    left = col < HEAD_DIM
    same = left == (row < HEAD_DIM)
    ones = jnp.where(same, 1.0, 0.0).astype(BF)
    length, width = o_ref.shape
    pairs = q_ref.shape[1] // PAIR

    def chunk(c, carry):
        rows = pl.ds(pl.multiple_of(c * CHUNK, CHUNK), CHUNK)
        for p in range(first, first + width // PAIR):
            lanes = slice(p * PAIR, (p + 1) * PAIR)
            place = slice((p - first) * PAIR, (p - first + 1) * PAIR)
            item = c * pairs + p
            query = silu(q_ref[rows, lanes].astype(F32))
            query = query * lax.rsqrt(half_sums(query * query, ones) + EPSILON)
            query = (query * HEAD_DIM ** (-0.5)).astype(BF)
            key_f = y_ref[item, :, 2 * PAIR :].astype(F32)
            owns = [jnp.where(left, key_f, 0.0), jnp.where(left, 0.0, key_f)]
            inside = dot_nt(query, jnp.concatenate(owns, axis=0).astype(BF))
            inside = (inside * d_ref[item].astype(F32)).astype(BF)
            got = halves(dot(inside, side_by_side(halves(y_ref[item, :, : 2 * PAIR]))))
            local = jnp.where(left, got[0], got[1])
            crossed = turned(jnp.where(left, got[1], got[0]))
            query = (query.astype(F32) * ec_ref[rows, lanes] - crossed).astype(BF)
            before = before_ref[item].astype(F32)
            both = [jnp.where(same, before, 0.0), jnp.where(same, turned(before), 0.0)]
            moved = halves(dot(query, jnp.concatenate(both, axis=1).astype(BF)))
            o_ref[rows, place] = local + moved[0]
            q1_ref[rows, place] = moved[1].astype(BF)
        return carry

    lax.fori_loop(0, length // CHUNK, chunk, 0)


def gates_side(gates, gain):
    return call(gates_kernel, [gates, gain.reshape(1, HEAD_DIM)], [(gates.shape, F32)])[0]


def queries_side(first, after, queries, decay, solved, before, grown):
    length, width = queries.shape
    shape = (length, width // 2)
    return call(
        functools.partial(queries_kernel, first),
        [queries, decay, solved, before, grown],
        [(shape, F32), (shape, BF)],
        far=[after],
    )


def chained(earlier, later, same):
    later = later.astype(F32)
    step = jnp.where(same, turned(later), 0.0).astype(BF)
    return dot(step, earlier.astype(BF)) + jnp.where(same, later, 0.0)


def chip_kernel(own_ref, other_ref, out_ref, kept_ref):
    kept_ref[...] = other_ref[...]
    row, col = places()
    same = (col < HEAD_DIM) == (row < HEAD_DIM)
    core = lax.axis_index(SP[2])
    count = out_ref.shape[0]
    for p in range(count):
        mine = own_ref[core * count + p]
        theirs = other_ref[core * count + p]
        first = jnp.where(core == 0, mine, theirs)
        second = jnp.where(core == 0, theirs, mine)
        out_ref[p] = chained(first, second, same).astype(BF)


def row_kernel(after_ref, *rest):
    parts, (total_ref, before_ref, all_ref) = rest[:-3], rest[-3:]
    row, col = places()
    same = (col < HEAD_DIM) == (row < HEAD_DIM)
    place = lax.axis_index(SP[1])
    size = len(parts)
    for k, part in enumerate(parts):
        all_ref[lax.rem(place - k + size, size)] = part[...]
    for p in range(total_ref.shape[0]):
        run = all_ref[0, p].astype(F32)
        inside = jnp.where(place == 0, jnp.where((row ^ col) == HEAD_DIM, 1.0, 0.0), run)
        for k in range(1, size):
            run = chained(run, all_ref[k, p], same)
            inside = jnp.where(k < place, run, inside)
        before_ref[p] = inside.astype(BF)
        total_ref[p] = run.astype(BF)


def plane_kernel(after_ref, before_ref, *rest):
    parts, out_ref = rest[:-1], rest[-1]
    row, col = places()
    same = (col < HEAD_DIM) == (row < HEAD_DIM)
    place = lax.axis_index(SP[0])
    for p in range(out_ref.shape[0]):
        state = jnp.zeros((PAIR, PAIR), F32)
        for k in range(len(parts), 0, -1):
            later = jnp.where(same, chained(state, parts[k - 1][p], same), 0.0)
            state = jnp.where(k <= place, later, state)
        state = chained(state, before_ref[p], same)
        out_ref[p] = jnp.where(same, state, 0.0).astype(BF)


def state_ahead(total, meanwhile, then):
    plane, line, core = SP
    swap = [(0, 1), (1, 0)]
    half = (total.shape[0] // 2, PAIR, PAIR)
    other = lax.ppermute(total, core, swap)
    chip, other = call(chip_kernel, [total, other], [(half, BF), (total.shape, BF)])
    size = lax.axis_size(line)
    lines = [chip] + [lax.ppermute(chip, line, ring(size, k)) for k in range(1, size)]
    early = meanwhile(chip)
    whole, before = call(
        row_kernel, lines, [(half, BF), (half, BF)], [pltpu.VMEM((size, *half), BF)], far=[early[1]]
    )
    size = lax.axis_size(plane)
    planes = [lax.ppermute(whole, plane, ring(size, k)) for k in range(1, size)]
    late = then(whole)
    (state,) = call(plane_kernel, [before] + planes, [(half, BF)], far=[late[1]])
    return early, late, (other, state, lax.ppermute(state, core, swap))


def mixed_kernel(
    o0_ref, q0_ref, o1_ref, q1_ref,
    first_ref, mine_ref, theirs_ref, gate_ref, w_ref, *rest,
):
    out_refs, (mixed_ref, state_ref) = rest[:-2], rest[-2:]
    row, col = places()
    same = (col < HEAD_DIM) == (row < HEAD_DIM)
    ones = jnp.where(same, 1.0, 0.0).astype(BF)
    length, width = gate_ref.shape
    size = len(out_refs)
    block = length // size
    core = lax.axis_index(SP[2])
    turn = lax.axis_index("tp")
    half = mine_ref.shape[0]
    state_ref[pl.ds(core * half, half)] = mine_ref[...]
    state_ref[pl.ds((1 - core) * half, half)] = theirs_ref[...]
    for p in range(width // PAIR):
        lanes = slice(p * PAIR, (p + 1) * PAIR)
        state = state_ref[p].astype(F32)
        later = jnp.where(same, chained(state, first_ref[p], same), 0.0)
        state = jnp.where(core == 0, state, later).astype(BF)
        o_ref, q_ref = ((o0_ref, q0_ref), (o1_ref, q1_ref))[p // half]
        place = slice((p % half) * PAIR, (p % half + 1) * PAIR)
        out = o_ref[:, place] + dot(q_ref[:, place], state)
        mean = half_sums(out * out, ones) * (1.0 / HEAD_DIM)
        out = (out * lax.rsqrt(mean + EPSILON) * gate_ref[:, lanes]).astype(BF)
        for k in range(size):
            start = pl.multiple_of(lax.rem(k - turn + size, size) * block, 32)
            mixed_ref[pl.ds(start, block), lanes] = out[k * block : (k + 1) * block, :]
    for n in range(w_ref.shape[1] // STRIP):
        here = slice(n * STRIP, (n + 1) * STRIP)
        got = dot(mixed_ref[...], w_ref[:, here])
        for k, out_ref in enumerate(out_refs):
            out_ref[:, here] = got[k * block : (k + 1) * block, :].astype(out_ref.dtype)


def mixed_and_projected(size, early, late, states, gate, w_out):
    length, width = gate.shape
    return call(
        mixed_kernel,
        [*early, *late, *states, gate, w_out],
        [((length // size, w_out.shape[1]), BF if k else F32) for k in range(size)],
        [pltpu.VMEM((length, width), BF), pltpu.VMEM((width // PAIR, PAIR, PAIR), BF)],
    )


def norm_kernel(stream_ref, gain_ref, *rest):
    parts, (middle_ref, normed_ref) = rest[:-2], rest[-2:]
    projected = parts[0][...]
    for part in parts[1:]:
        projected = projected + part[...].astype(F32)
    middle = (stream_ref[...].astype(F32) + projected).astype(BF)
    middle_ref[...] = middle
    middle = middle.astype(F32)
    mean = jnp.mean(middle * middle, axis=-1, keepdims=True)
    normed_ref[...] = (middle * lax.rsqrt(mean + EPSILON) * gain_ref[...]).astype(BF)


def normed_rows(stream, gain, parts):
    return call(
        norm_kernel, [stream, gain.reshape(1, -1), *parts], [(stream.shape, BF), (stream.shape, BF)]
    )


def activated(rows, gate, up):
    got = dot(rows, jnp.concatenate([gate, up], axis=1))
    width = gate.shape[1]
    return (silu(got[:, :width]) * got[:, width:]).astype(BF)


def product_nt(a, b):
    even = a.shape[1] // 256 * 256
    return dot_nt(a[:, :even], b[:, :even]) + dot_nt(a[:, even:], b[:, even:])


TILE = 128
STRIP = 256
AHEAD = 3
UP_GROUPS = (3, 5, 3)
DOWN_GROUPS = (5, 3)


def first_channels_kernel(w_ref, across_ref, right_ref, left_ref, *rest):
    out_refs, kept_ref = rest[:2], rest[2]
    gate_ref, up_ref, down_ref, hidden_ref, in_sems, down_sems = rest[3:]
    width, hidden = gate_ref.shape
    block = out_refs[0].shape[0]
    rows = across_ref.shape[0]
    groups, spans = [], []
    for many, spread in ((hidden // TILE, UP_GROUPS), (width // STRIP, DOWN_GROUPS)):
        assert sum(spread) == many
        starts = [sum(spread[:k]) for k in range(len(spread))]
        spans.append([range(start, start + n) for start, n in zip(starts, spread)])
    for g, tiles in enumerate(spans[0]):
        here = pl.ds(tiles[0] * TILE, len(tiles) * TILE)
        group = []
        for k, ref in enumerate((gate_ref, up_ref)):
            from_ref = w_ref.at[:, pl.ds(k * hidden + tiles[0] * TILE, len(tiles) * TILE)]
            group.append(pltpu.make_async_copy(from_ref, ref.at[:, here], in_sems.at[k, g]))
        groups.append(group)
    for g, strips in enumerate(spans[1]):
        here = pl.ds(strips[0] * STRIP, len(strips) * STRIP)
        from_ref = w_ref.at[here, pl.ds(2 * hidden, hidden)]
        groups.append([pltpu.make_async_copy(from_ref, down_ref.at[here, :], down_sems.at[g])])

    def begin(g):
        if g < len(groups):
            for copy in groups[g]:
                copy.start()

    def arrived(g):
        for copy in groups[g]:
            copy.wait()
        begin(g + AHEAD)

    for g in range(AHEAD):
        begin(g)
    for g, tiles in enumerate(spans[0]):
        arrived(g)
        for j in tiles:
            here = slice(j * TILE, (j + 1) * TILE)
            every = [across_ref[...], right_ref[...], left_ref[...]]
            every = jnp.concatenate(every, axis=0)
            units = activated(every, gate_ref[:, here], up_ref[:, here])
            hidden_ref[:, here] = units[:rows, :]
            kept_ref[:, here] = units[rows:, :]
    for g, strips in enumerate(spans[1]):
        arrived(len(spans[0]) + g)
        for n in strips:
            here = slice(n * STRIP, (n + 1) * STRIP)
            got = product_nt(hidden_ref[...], down_ref[here, :])
            for k, out_ref in enumerate(out_refs):
                out_ref[:, here] = got[k * block : (k + 1) * block, :].astype(BF)


def first_channels(weights, across, right, left, hidden):
    block, width = across.shape
    half = ((block // 2, width), BF)
    out = call(
        first_channels_kernel,
        [across, right, left],
        [half, half, ((2 * block, hidden), BF)] + [((width, hidden), BF)] * 3,
        [
            pltpu.VMEM((block, hidden), BF),
            pltpu.SemaphoreType.DMA((2, len(UP_GROUPS))),
            pltpu.SemaphoreType.DMA((len(DOWN_GROUPS),)),
        ],
        far=[pltpu.with_memory_space_constraint(weights, pltpu.HBM)],
    )
    return out[:2], out[2], out[3:]


def neighbours_kernel(hidden_ref, down_ref, *out_refs):
    half = out_refs[0].shape[0]
    for n in range(down_ref.shape[0] // STRIP):
        here = slice(n * STRIP, (n + 1) * STRIP)
        got = product_nt(hidden_ref[...], down_ref[here, :]).astype(BF)
        for k, out_ref in enumerate(out_refs):
            out_ref[:, here] = got[k * half : (k + 1) * half, :]


def neighbours(hidden, down):
    shape = (hidden.shape[0] // 4, down.shape[0])
    return call(neighbours_kernel, [hidden, down], [(shape, BF)] * 4)


def more_channels_kernel(count, *refs):
    parts, (gate_ref, up_ref, down_ref) = refs[:count], refs[count : count + 3]
    out_refs, hidden_ref = refs[count + 3 : -1], refs[-1]
    block = parts[0].shape[0]
    rows = jnp.concatenate([part[...] for part in parts], axis=0)
    for j in range(gate_ref.shape[1] // TILE):
        here = slice(j * TILE, (j + 1) * TILE)
        hidden_ref[:, here] = activated(rows, gate_ref[:, here], up_ref[:, here])
    for n in range(down_ref.shape[0] // STRIP):
        here = slice(n * STRIP, (n + 1) * STRIP)
        got = product_nt(hidden_ref[...], down_ref[here, :])
        for k, out_ref in enumerate(out_refs):
            out_ref[:, here] = got[k * block : (k + 1) * block, :].astype(BF)


def more_channels(rows, projections):
    block, width = rows[0].shape
    count = len(rows)
    return call(
        functools.partial(more_channels_kernel, count),
        [*rows, *projections],
        [((block, width), BF)] * count,
        [pltpu.VMEM((count * block, projections[0].shape[1]), BF)],
    )


def joined_kernel(low_ref, more_low_ref, high_ref, more_high_ref, low_out_ref, high_out_ref):
    low = low_ref[...].astype(F32) + more_low_ref[...].astype(F32)
    low_out_ref[...] = low.astype(BF)
    high = high_ref[...].astype(F32) + more_high_ref[...].astype(F32)
    high_out_ref[...] = high.astype(BF)


def joined(low, more_low, high, more_high):
    shapes = [(low.shape, BF)] * 2
    return call(joined_kernel, [low, more_low, high, more_high], shapes)


def last_kernel(middle_ref, own_ref, *rest):
    parts, out_ref = rest[:-1], rest[-1]
    half = parts[0].shape[0]
    for k in range(2):
        rows = slice(k * half, (k + 1) * half)
        total = own_ref[rows, :].astype(F32)
        for part in parts[2 * k : 2 * k + 2]:
            total = total + part[...].astype(F32)
        out_ref[rows, :] = (middle_ref[rows, :].astype(F32) + 0.5 * total).astype(BF)


def last_sum(middle, parts):
    near = [pltpu.with_memory_space_constraint(x, pltpu.VMEM) for x in [middle, *parts]]
    return pl.pallas_call(
        last_kernel,
        in_specs=[FULL] * len(near),
        out_specs=FULL,
        out_shape=jax.ShapeDtypeStruct(middle.shape, BF),
        compiler_params=pltpu.CompilerParams(vmem_limit_bytes=16 << 20),
        name="last_sum",
    )(*near)


def per_device(
    queries,
    keys,
    values,
    gates,
    decay_pre,
    beta_pre,
    out_gain,
    w_out,
    stream,
    norm_gain,
    w_gate,
    w_up,
    w_down,
):
    hidden = w_gate.shape[1]
    weights = jnp.concatenate([w_gate, w_up, w_down.T], axis=1)
    weights = lax.all_gather(weights, SP, axis=0, tiled=True)
    size = lax.axis_size("tp")
    before, total, solved, decay, grown = keys_side(keys, values, beta_pre, decay_pre)
    gate = gates_side(gates, out_gain)
    pairs = queries.shape[1] // PAIR
    early, late, states = state_ahead(
        total,
        lambda x: queries_side(0, x, queries, decay, solved, before, grown),
        lambda x: queries_side(pairs // 2, x, queries, decay, solved, before, grown),
    )
    parts = mixed_and_projected(size, early, late, states, gate, w_out)
    parts = [parts[0]] + [lax.ppermute(parts[k], "tp", ring(size, k)) for k in (1, 2, 3)]
    middle, normed = normed_rows(stream, norm_gain, parts)
    across = lax.ppermute(normed, "tp", ring(size, 2))
    right = lax.ppermute(normed, "tp", ring(size, 1))
    left = lax.ppermute(normed, "tp", ring(size, -1))
    far, units, projections = first_channels(weights, across, right, left, hidden)
    upper = lax.ppermute(far[0], "tp", ring(size, 1))
    lower = lax.ppermute(far[1], "tp", ring(size, -1))
    right_up, right_low, left_up, left_low = neighbours(units, projections[2])
    right_up = lax.ppermute(right_up, "tp", ring(size, -1))
    left_low = lax.ppermute(left_low, "tp", ring(size, 1))
    right_low, left_up = joined(right_low, lower, left_up, upper)
    right_low = lax.ppermute(right_low, "tp", ring(size, -1))
    left_up = lax.ppermute(left_up, "tp", ring(size, 1))
    (own,) = more_channels([normed], projections)
    return last_sum(middle, [own, right_up, left_up, right_low, left_low])


def solution(mesh):
    finer = Mesh(mesh.devices.reshape(4, 4, 2, mesh.shape["tp"]), SP_TP)
    placed = (
        P(SP, "tp"),
        P(SP, "tp"),
        P(SP, "tp"),
        P(SP, "tp"),
        P("tp", SP),
        P("tp", SP),
        P(),
        P("tp", None),
        P(SP_TP, None),
        P(),
        P(SP, "tp"),
        P(SP, "tp"),
        P("tp", SP),
    )
    return jax.shard_map(
        per_device, mesh=finer, in_specs=placed, out_specs=P(SP_TP, None), check_vma=False
    )
```

profile of v0, /device:TPU:0, one launch (start us, length us, event | category | flops | bytes accessed | tf_op | source)
XLA Modules:
  0.0 125.7 jit_solution(8852876889271536255)
XLA Ops:
  6.5 2.0 %pad_maximum_fusion = bf16[64,4224]{1,0:T(8,128)(2,1)} fusion(bf16[64,1408]{1,0:T(8,128)(2,1)} %bitcast.5, bf16[64,1408]{1,0:T(8,128)(2,1)} %param.24, bf16[64,1408]{1,0:T(8,128)(2,1)} %param.23), kind=kLoop, calls=%fused_computation | loop fusion | flops 1622016 | bytes 1081344 | tf_op jit(solution)/shard_map/concatenate | solution.py:614
  8.5 0.0 all-gather.2.cloned.1.call-update
  8.6 8.1 %shard_map.127 = (bf16[12,128,128]{2,1,0:T(8,128)(2,1)S(1)}, bf16[4,128,128]{2,1,0:T(8,128)(2,1)S(1)}, bf16[12,128,384]{2,1,0:T(8,128)(2,1)S(1)}, bf16[12,128,256]{2,1,0:T(8,128)(2,1)S(1)}, f32[384,512]{1,0:T(8,128)S(1)}) custom-call(bf16[384,512]{1,0:T(8,128)(2,1)} %k_far_ref.1, bf16[384,512]{1,0:T(8,128)(2,1)} %v_far_ref.1, f32[8,384]{1,0:T(8,128)} %beta_far_ref.1, ...), custom_call_target="tpu_custom_call" | custom-call | tf_op jit(solution)/shard_map/pallas_call | solution.py:29
  16.6 0.1 collective-permute-start
  16.7 1.3 %collective-permute-done.other_ref = bf16[4,128,128]{2,1,0:T(8,128)(2,1)S(1)} collective-permute-done((bf16[4,128,128]{2,1,0:T(8,128)(2,1)S(1)}, bf16[4,128,128]{2,1,0:T(8,128)(2,1)S(1)}, u32[]{:S(2)}, u32[]{:S(2)}) %collective-permute-start) | collective-permute-done | bytes 131104 | tf_op jit(solution)/shard_map/ppermute | solution.py:356
  18.1 0.2 shard_map.128
  18.3 3.2 %collective-permute-start.3 = (bf16[2,128,128]{2,1,0:T(8,128)(2,1)S(1)}, bf16[2,128,128]{2,1,0:T(8,128)(2,1)S(1)}, u32[]{:S(2)}, u32[]{:S(2)}) collective-permute-start(bf16[2,128,128]{2,1,0:T(8,128)(2,1)S(1)} %get-tuple-element.37.after_ref.rest_0_), channel_id=1, source_target_pairs={{0,24},{8,0},{16,8},{24,16},{1,25},{9,1},{17,9},{25,17},{2,26},{10... | collective-permute-start | bytes 196616 | tf_op jit(solution)/shard_map/ppermute | solution.py:359
  21.5 0.6 collective-permute-start.2
  22.1 1.0 collective-permute-start.1
  23.1 2.9 %shard_map.129 = (f32[384,256]{1,0:T(8,128)S(1)}, bf16[384,256]{1,0:T(8,128)(2,1)S(1)}) custom-call(bf16[2,128,128]{2,1,0:T(8,128)(2,1)S(1)} %get-tuple-element.37.after_ref.rest_0_, bf16[384,512]{1,0:T(8,128)(2,1)S(1)} %copy-done.1, bf16[12,128,256]{2,1,0:T(8,128)(2,1)S(1)} %get-tuple-element.38.d_ref, bf16[12,128,384]{2,1,0:T(8,128)(2,1)S(1)} %get-tuple-element.39.y_ref, ...), custom_call_target="tpu_custom_call" | custom-call | tf_op jit(solution)/shard_map/pallas_call | solution.py:29
  26.0 2.9 %collective-permute-done.2.rest_2_ = bf16[2,128,128]{2,1,0:T(8,128)(2,1)S(1)} collective-permute-done((bf16[2,128,128]{2,1,0:T(8,128)(2,1)S(1)}, bf16[2,128,128]{2,1,0:T(8,128)(2,1)S(1)}, u32[]{:S(2)}, u32[]{:S(2)}) %collective-permute-start.2) | collective-permute-done | bytes 65568 | tf_op jit(solution)/shard_map/ppermute | solution.py:359
  28.9 0.9 collective-permute-done.1.rest_1_
  29.8 0.6 shard_map.130
  30.5 0.0 copy-start.3
  30.5 4.5 %collective-permute-start.6 = (bf16[2,128,128]{2,1,0:T(8,128)(2,1)S(1)}, bf16[2,128,128]{2,1,0:T(8,128)(2,1)S(1)}, u32[]{:S(2)}, u32[]{:S(2)}) collective-permute-start(bf16[2,128,128]{2,1,0:T(8,128)(2,1)S(1)} %get-tuple-element.44.after_ref), channel_id=1, source_target_pairs={{0,96},{32,0},{64,32},{96,64},{1,97},{33,1},{65,33},{97,65},{2,98}... | collective-permute-start | bytes 196616 | tf_op jit(solution)/shard_map/ppermute | solution.py:365
  35.0 1.2 collective-permute-start.4
  36.1 2.9 %shard_map.131 = (f32[384,256]{1,0:T(8,128)S(1)}, bf16[384,256]{1,0:T(8,128)(2,1)S(1)}) custom-call(bf16[2,128,128]{2,1,0:T(8,128)(2,1)S(1)} %get-tuple-element.44.after_ref, bf16[384,512]{1,0:T(8,128)(2,1)S(1)} %copy-done.1, bf16[12,128,256]{2,1,0:T(8,128)(2,1)S(1)} %get-tuple-element.38.d_ref, bf16[12,128,384]{2,1,0:T(8,128)(2,1)S(1)} %get-tuple-element.39.y_ref, ...), custom_call_target="tpu_custom_call" | custom-call | tf_op jit(solution)/shard_map/pallas_call | solution.py:29
  39.1 3.1 %collective-permute-done.5.rest_1_ = bf16[2,128,128]{2,1,0:T(8,128)(2,1)S(1)} collective-permute-done((bf16[2,128,128]{2,1,0:T(8,128)(2,1)S(1)}, bf16[2,128,128]{2,1,0:T(8,128)(2,1)S(1)}, u32[]{:S(2)}, u32[]{:S(2)}) %collective-permute-start.5) | collective-permute-done | bytes 65568 | tf_op jit(solution)/shard_map/ppermute | solution.py:365
  42.1 0.3 collective-permute-done.4.rest_0_
  42.5 0.9 shard_map.132.mine_ref
  43.4 0.3 collective-permute-start.7
  43.6 0.3 shard_map.133.gate_ref
  43.9 0.9 collective-permute-done.7.theirs_ref
  44.9 2.1 %shard_map.134 = (f32[96,2048]{1,0:T(8,128)S(1)}, bf16[96,2048]{1,0:T(8,128)(2,1)S(1)}, bf16[96,2048]{1,0:T(8,128)(2,1)S(1)}, bf16[96,2048]{1,0:T(8,128)(2,1)S(1)}) custom-call(f32[384,256]{1,0:T(8,128)S(1)} %get-tuple-element.42.o0_ref, bf16[384,256]{1,0:T(8,128)(2,1)S(1)} %get-tuple-element.43.after_ref.q0_ref, f32[384,256]{1,0:T(8,128)S(1)} %get-tuple-element.45.o1_ref, ...), custom_call_target="tpu_custom_call" | custom-call | tf_op jit(solution)/shard_map/pallas_call | solution.py:29
  47.0 1.6 %collective-permute-start.8 = (bf16[96,2048]{1,0:T(8,128)(2,1)S(1)}, bf16[96,2048]{1,0:T(8,128)(2,1)S(1)}, u32[]{:S(2)}, u32[]{:S(2)}) collective-permute-start(bf16[96,2048]{1,0:T(8,128)(2,1)S(1)} %get-tuple-element.50), channel_id=1, source_target_pairs={{0,1},{1,2},{2,3},{3,0},{4,5},{5,6},{6,7},{7,4},{8,9},{9,10},{10,1... | collective-permute-start | bytes 1179656 | tf_op jit(solution)/shard_map/ppermute | solution.py:626
  48.6 2.6 %collective-permute-start.9 = (bf16[96,2048]{1,0:T(8,128)(2,1)S(1)}, bf16[96,2048]{1,0:T(8,128)(2,1)S(1)}, u32[]{:S(2)}, u32[]{:S(2)}) collective-permute-start(bf16[96,2048]{1,0:T(8,128)(2,1)S(1)} %get-tuple-element.51), channel_id=1, source_target_pairs={{0,2},{1,3},{2,0},{3,1},{4,6},{5,7},{6,4},{7,5},{8,10},{9,11},{10,... | collective-permute-start | bytes 1179656 | tf_op jit(solution)/shard_map/ppermute | solution.py:626
  51.3 1.5 %collective-permute-start.10 = (bf16[96,2048]{1,0:T(8,128)(2,1)S(1)}, bf16[96,2048]{1,0:T(8,128)(2,1)S(1)}, u32[]{:S(2)}, u32[]{:S(2)}) collective-permute-start(bf16[96,2048]{1,0:T(8,128)(2,1)S(1)} %get-tuple-element.52), channel_id=1, source_target_pairs={{0,3},{1,0},{2,1},{3,2},{4,7},{5,4},{6,5},{7,6},{8,11},{9,8},{10,9... | collective-permute-start | bytes 1179656 | tf_op jit(solution)/shard_map/ppermute | solution.py:626
  52.7 6.7 %collective-permute-done.8.rest_1_ = bf16[96,2048]{1,0:T(8,128)(2,1)S(1)} collective-permute-done((bf16[96,2048]{1,0:T(8,128)(2,1)S(1)}, bf16[96,2048]{1,0:T(8,128)(2,1)S(1)}, u32[]{:S(2)}, u32[]{:S(2)}) %collective-permute-start.8) | collective-permute-done | bytes 393248 | tf_op jit(solution)/shard_map/ppermute | solution.py:626
  59.5 9.4 %collective-permute-done.9.rest_2_ = bf16[96,2048]{1,0:T(8,128)(2,1)S(1)} collective-permute-done((bf16[96,2048]{1,0:T(8,128)(2,1)S(1)}, bf16[96,2048]{1,0:T(8,128)(2,1)S(1)}, u32[]{:S(2)}, u32[]{:S(2)}) %collective-permute-start.9) | collective-permute-done | bytes 393248 | tf_op jit(solution)/shard_map/ppermute | solution.py:626
  68.8 0.4 shard_map.135
  69.3 2.4 %collective-permute-start.13 = (bf16[96,2048]{1,0:T(8,128)(2,1)S(1)}, bf16[96,2048]{1,0:T(8,128)(2,1)S(1)}, u32[]{:S(2)}, u32[]{:S(2)}) collective-permute-start(bf16[96,2048]{1,0:T(8,128)(2,1)S(1)} %get-tuple-element.54.refs_0_), channel_id=1, source_target_pairs={{0,3},{1,0},{2,1},{3,2},{4,7},{5,4},{6,5},{7,6},{8,11},{9,8},{10,9... | collective-permute-start | bytes 1179656 | tf_op jit(solution)/shard_map/ppermute | solution.py:630
  71.7 2.4 %collective-permute-start.11 = (bf16[96,2048]{1,0:T(8,128)(2,1)S(1)}, bf16[96,2048]{1,0:T(8,128)(2,1)S(1)}, u32[]{:S(2)}, u32[]{:S(2)}) collective-permute-start(bf16[96,2048]{1,0:T(8,128)(2,1)S(1)} %get-tuple-element.54.refs_0_), channel_id=1, source_target_pairs={{0,2},{1,3},{2,0},{3,1},{4,6},{5,7},{6,4},{7,5},{8,10},{9,11},{10,... | collective-permute-start | bytes 1179656 | tf_op jit(solution)/shard_map/ppermute | solution.py:628
  74.1 14.7 %collective-permute-done.13.left_ref = bf16[96,2048]{1,0:T(8,128)(2,1)S(1)} collective-permute-done((bf16[96,2048]{1,0:T(8,128)(2,1)S(1)}, bf16[96,2048]{1,0:T(8,128)(2,1)S(1)}, u32[]{:S(2)}, u32[]{:S(2)}) %collective-permute-start.13) | collective-permute-done | bytes 393248 | tf_op jit(solution)/shard_map/ppermute | solution.py:630
  88.8 3.4 %collective-permute-done.12.right_ref = bf16[96,2048]{1,0:T(8,128)(2,1)S(1)} collective-permute-done((bf16[96,2048]{1,0:T(8,128)(2,1)S(1)}, bf16[96,2048]{1,0:T(8,128)(2,1)S(1)}, u32[]{:S(2)}, u32[]{:S(2)}) %collective-permute-start.12) | collective-permute-done | bytes 393248 | tf_op jit(solution)/shard_map/ppermute | solution.py:629
  92.2 9.3 %shard_map.136 = (bf16[48,2048]{1,0:T(8,128)(2,1)S(1)}, bf16[48,2048]{1,0:T(8,128)(2,1)S(1)}, bf16[192,1408]{1,0:T(8,128)(2,1)S(1)}, bf16[2048,1408]{1,0:T(8,128...) custom-call(bf16[2048,4224]{1,0:T(8,128)(2,1)} %all-gather.2.cloned.1.call-done.w_ref, ...), custom_call_target="tpu_custom_call" | custom-call | tf_op jit(solution)/shard_map/pallas_call | solution.py:29
  101.5 0.4 collective-permute-start.15
  101.9 1.7 %collective-permute-start.16 = (bf16[48,2048]{1,0:T(8,128)(2,1)S(1)}, bf16[48,2048]{1,0:T(8,128)(2,1)S(1)}, u32[]{:S(2)}, u32[]{:S(2)}) collective-permute-start(bf16[48,2048]{1,0:T(8,128)(2,1)S(1)} %get-tuple-element.63), channel_id=1, source_target_pairs={{0,1},{1,2},{2,3},{3,0},{4,5},{5,6},{6,7},{7,4},{8,9},{9,10},{10,1... | collective-permute-start | bytes 589832 | tf_op jit(solution)/shard_map/ppermute | solution.py:632
  103.6 2.0 %shard_map.138 = (bf16[48,2048]{1,0:T(8,128)(2,1)S(1)}, bf16[48,2048]{1,0:T(8,128)(2,1)S(1)}, bf16[48,2048]{1,0:T(8,128)(2,1)S(1)}, bf16[48,2048]{1,0:T(8,128)(2,1)S(1)}) custom-call(bf16[192,1408]{1,0:T(8,128)(2,1)S(1)} %get-tuple-element.58.hidden_ref, bf16[2048,1408]{1,0:T(8,128)(2,1)S(1)} %get-tuple-element.57.refs_3_.down_ref), custom_call_target="tpu_custom_call" | custom-call | tf_op jit(solution)/shard_map/pallas_call | solution.py:29
  105.6 1.6 %collective-permute-start.14 = (bf16[48,2048]{1,0:T(8,128)(2,1)S(1)}, bf16[48,2048]{1,0:T(8,128)(2,1)S(1)}, u32[]{:S(2)}, u32[]{:S(2)}) collective-permute-start(bf16[48,2048]{1,0:T(8,128)(2,1)S(1)} %get-tuple-element.59), channel_id=1, source_target_pairs={{0,3},{1,0},{2,1},{3,2},{4,7},{5,4},{6,5},{7,6},{8,11},{9,8},{10,9... | collective-permute-start | bytes 589832 | tf_op jit(solution)/shard_map/ppermute | solution.py:635
  107.2 0.5 collective-permute-start.19
  107.7 0.2 collective-permute-done.15.more_low_ref
  108.0 0.9 collective-permute-done.16.more_high_ref
  108.9 0.1 shard_map.139
  109.0 1.1 collective-permute-start.17
  110.1 2.2 %collective-permute-start.18 = (bf16[48,2048]{1,0:T(8,128)(2,1)S(1)}, bf16[48,2048]{1,0:T(8,128)(2,1)S(1)}, u32[]{:S(2)}, u32[]{:S(2)}) collective-permute-start(bf16[48,2048]{1,0:T(8,128)(2,1)S(1)} %get-tuple-element.65), channel_id=1, source_target_pairs={{0,3},{1,0},{2,1},{3,2},{4,7},{5,4},{6,5},{7,6},{8,11},{9,8},{10,9... | collective-permute-start | bytes 589832 | tf_op jit(solution)/shard_map/ppermute | solution.py:638
  112.3 4.0 %shard_map.137.own_ref = bf16[96,2048]{1,0:T(8,128)(2,1)S(1)} custom-call(bf16[96,2048]{1,0:T(8,128)(2,1)S(1)} %get-tuple-element.54.refs_0_, bf16[2048,1408]{1,0:T(8,128)(2,1)S(1)} %get-tuple-element.55.refs_1_, bf16[2048,1408]{1,0:T(8,128)(2,1)S(1)} %get-tuple-element.56.refs_2_, bf16[2048,1408]{1,0:T(8,128)(2,1)S(1)} %get-tuple-element.57.refs_3_.down_ref), custom_call_target="tpu_custom_call" | custom-call | tf_op jit(solution)/shard_map/pallas_call | solution.py:29
  116.3 1.6 %collective-permute-done.17.rest_1_ = bf16[48,2048]{1,0:T(8,128)(2,1)S(1)} collective-permute-done((bf16[48,2048]{1,0:T(8,128)(2,1)S(1)}, bf16[48,2048]{1,0:T(8,128)(2,1)S(1)}, u32[]{:S(2)}, u32[]{:S(2)}) %collective-permute-start.17) | collective-permute-done | bytes 196640 | tf_op jit(solution)/shard_map/ppermute | solution.py:639
  117.9 1.0 last_sum.1
  (22 shorter events, 0.1 us)
Async XLA Ops:
  6.5 85.6 %all-gather.2.cloned.1.call-start = ((), (), s32[]{:S(2)}) async-start(), calls=%async_computation | async-start | bytes 17842176 | tf_op jit(solution)/shard_map/all_gather | solution.py:615
  6.5 16.5 %copy-start.1 = (bf16[384,512]{1,0:T(8,128)(2,1)S(1)}, bf16[384,512]{1,0:T(8,128)(2,1)}, u32[]{:S(2)}) copy-start(bf16[384,512]{1,0:T(8,128)(2,1)} %q_ref.3) | copy-start | bytes 1179652
  16.6 1.4 %collective-permute-start = (bf16[4,128,128]{2,1,0:T(8,128)(2,1)S(1)}, bf16[4,128,128]{2,1,0:T(8,128)(2,1)S(1)}, u32[]{:S(2)}, u32[]{:S(2)}) collective-permute-start(bf16[4,128,128]{2,1,0:T(8,128)(2,1)S(1)} %get-tuple-element.36.own_ref), channel_id=1, source_target_pairs={{0,4},{4,0},{1,5},{5,1},{2,6},{6,2},{3,7},{7,3},{8,12},{12,8},{9,1... | collective-permute-start | bytes 393224 | tf_op jit(solution)/shard_map/ppermute | solution.py:356
  18.3 7.7 %collective-permute-start.3 = (bf16[2,128,128]{2,1,0:T(8,128)(2,1)S(1)}, bf16[2,128,128]{2,1,0:T(8,128)(2,1)S(1)}, u32[]{:S(2)}, u32[]{:S(2)}) collective-permute-start(bf16[2,128,128]{2,1,0:T(8,128)(2,1)S(1)} %get-tuple-element.37.after_ref.rest_0_), channel_id=1, source_target_pairs={{0,24},{8,0},{16,8},{24,16},{1,25},{9,1},{17,9},{25,17},{2,26},{10... | collective-permute-start | bytes 196616 | tf_op jit(solution)/shard_map/ppermute | solution.py:359
  21.5 7.4 %collective-permute-start.2 = (bf16[2,128,128]{2,1,0:T(8,128)(2,1)S(1)}, bf16[2,128,128]{2,1,0:T(8,128)(2,1)S(1)}, u32[]{:S(2)}, u32[]{:S(2)}) collective-permute-start(bf16[2,128,128]{2,1,0:T(8,128)(2,1)S(1)} %get-tuple-element.37.after_ref.rest_0_), channel_id=1, source_target_pairs={{0,16},{8,24},{16,0},{24,8},{1,17},{9,25},{17,1},{25,9},{2,18},{10... | collective-permute-start | bytes 196616 | tf_op jit(solution)/shard_map/ppermute | solution.py:359
  22.1 7.7 %collective-permute-start.1 = (bf16[2,128,128]{2,1,0:T(8,128)(2,1)S(1)}, bf16[2,128,128]{2,1,0:T(8,128)(2,1)S(1)}, u32[]{:S(2)}, u32[]{:S(2)}) collective-permute-start(bf16[2,128,128]{2,1,0:T(8,128)(2,1)S(1)} %get-tuple-element.37.after_ref.rest_0_), channel_id=1, source_target_pairs={{0,8},{8,16},{16,24},{24,0},{1,9},{9,17},{17,25},{25,1},{2,10},{10... | collective-permute-start | bytes 196616 | tf_op jit(solution)/shard_map/ppermute | solution.py:359
  30.5 13.2 %copy-start.3 = (bf16[384,512]{1,0:T(8,128)(2,1)S(1)}, bf16[384,512]{1,0:T(8,128)(2,1)}, u32[]{:S(2)}) copy-start(bf16[384,512]{1,0:T(8,128)(2,1)} %gates_ref.1) | copy-start | bytes 1179652
  30.5 13.2 %copy-start.5 = (f32[64]{0:T(128)S(1)}, f32[64]{0:T(128)}, u32[]{:S(2)}) copy-start(f32[64]{0:T(128)} %param.19) | copy-start | bytes 772
  30.5 8.6 %collective-permute-start.6 = (bf16[2,128,128]{2,1,0:T(8,128)(2,1)S(1)}, bf16[2,128,128]{2,1,0:T(8,128)(2,1)S(1)}, u32[]{:S(2)}, u32[]{:S(2)}) collective-permute-start(bf16[2,128,128]{2,1,0:T(8,128)(2,1)S(1)} %get-tuple-element.44.after_ref), channel_id=1, source_target_pairs={{0,96},{32,0},{64,32},{96,64},{1,97},{33,1},{65,33},{97,65},{2,98}... | collective-permute-start | bytes 196616 | tf_op jit(solution)/shard_map/ppermute | solution.py:365
  35.0 7.2 %collective-permute-start.5 = (bf16[2,128,128]{2,1,0:T(8,128)(2,1)S(1)}, bf16[2,128,128]{2,1,0:T(8,128)(2,1)S(1)}, u32[]{:S(2)}, u32[]{:S(2)}) collective-permute-start(bf16[2,128,128]{2,1,0:T(8,128)(2,1)S(1)} %get-tuple-element.44.after_ref), channel_id=1, source_target_pairs={{0,64},{32,96},{64,0},{96,32},{1,65},{33,97},{65,1},{97,33},{2,66}... | collective-permute-start | bytes 196616 | tf_op jit(solution)/shard_map/ppermute | solution.py:365
  35.0 7.5 %collective-permute-start.4 = (bf16[2,128,128]{2,1,0:T(8,128)(2,1)S(1)}, bf16[2,128,128]{2,1,0:T(8,128)(2,1)S(1)}, u32[]{:S(2)}, u32[]{:S(2)}) collective-permute-start(bf16[2,128,128]{2,1,0:T(8,128)(2,1)S(1)} %get-tuple-element.44.after_ref), channel_id=1, source_target_pairs={{0,32},{32,64},{64,96},{96,0},{1,33},{33,65},{65,97},{97,1},{2,34}... | collective-permute-start | bytes 196616 | tf_op jit(solution)/shard_map/ppermute | solution.py:365
  36.1 8.7 %copy-start = (bf16[512,2048]{1,0:T(8,128)(2,1)S(1)}, bf16[512,2048]{1,0:T(8,128)(2,1)}, u32[]{:S(2)}) copy-start(bf16[512,2048]{1,0:T(8,128)(2,1)} %w_ref.1) | copy-start | bytes 6291460
  43.4 1.5 %collective-permute-start.7 = (bf16[2,128,128]{2,1,0:T(8,128)(2,1)S(1)}, bf16[2,128,128]{2,1,0:T(8,128)(2,1)S(1)}, u32[]{:S(2)}, u32[]{:S(2)}) collective-permute-start(bf16[2,128,128]{2,1,0:T(8,128)(2,1)S(1)} %shard_map.132.mine_ref), channel_id=1, source_target_pairs={{0,4},{4,0},{1,5},{5,1},{2,6},{6,2},{3,7},{7,3},{8,12},{12,8},{9,1... | collective-permute-start | bytes 196616 | tf_op jit(solution)/shard_map/ppermute | solution.py:368
  44.9 24.0 %copy-start.2 = (bf16[96,2048]{1,0:T(8,128)(2,1)S(1)}, bf16[96,2048]{1,0:T(8,128)(2,1)}, u32[]{:S(2)}) copy-start(bf16[96,2048]{1,0:T(8,128)(2,1)} %stream_ref.1) | copy-start | bytes 1179652
  44.9 24.0 %copy-start.4 = (f32[2048]{0:T(1024)S(1)}, f32[2048]{0:T(1024)}, u32[]{:S(2)}) copy-start(f32[2048]{0:T(1024)} %param.22) | copy-start | bytes 24580
  47.0 12.5 %collective-permute-start.8 = (bf16[96,2048]{1,0:T(8,128)(2,1)S(1)}, bf16[96,2048]{1,0:T(8,128)(2,1)S(1)}, u32[]{:S(2)}, u32[]{:S(2)}) collective-permute-start(bf16[96,2048]{1,0:T(8,128)(2,1)S(1)} %get-tuple-element.50), channel_id=1, source_target_pairs={{0,1},{1,2},{2,3},{3,0},{4,5},{5,6},{6,7},{7,4},{8,9},{9,10},{10,1... | collective-permute-start | bytes 1179656 | tf_op jit(solution)/shard_map/ppermute | solution.py:626
  48.6 20.2 %collective-permute-start.9 = (bf16[96,2048]{1,0:T(8,128)(2,1)S(1)}, bf16[96,2048]{1,0:T(8,128)(2,1)S(1)}, u32[]{:S(2)}, u32[]{:S(2)}) collective-permute-start(bf16[96,2048]{1,0:T(8,128)(2,1)S(1)} %get-tuple-element.51), channel_id=1, source_target_pairs={{0,2},{1,3},{2,0},{3,1},{4,6},{5,7},{6,4},{7,5},{8,10},{9,11},{10,... | collective-permute-start | bytes 1179656 | tf_op jit(solution)/shard_map/ppermute | solution.py:626
  51.3 17.6 %collective-permute-start.10 = (bf16[96,2048]{1,0:T(8,128)(2,1)S(1)}, bf16[96,2048]{1,0:T(8,128)(2,1)S(1)}, u32[]{:S(2)}, u32[]{:S(2)}) collective-permute-start(bf16[96,2048]{1,0:T(8,128)(2,1)S(1)} %get-tuple-element.52), channel_id=1, source_target_pairs={{0,3},{1,0},{2,1},{3,2},{4,7},{5,4},{6,5},{7,6},{8,11},{9,8},{10,9... | collective-permute-start | bytes 1179656 | tf_op jit(solution)/shard_map/ppermute | solution.py:626
  69.3 19.5 %collective-permute-start.13 = (bf16[96,2048]{1,0:T(8,128)(2,1)S(1)}, bf16[96,2048]{1,0:T(8,128)(2,1)S(1)}, u32[]{:S(2)}, u32[]{:S(2)}) collective-permute-start(bf16[96,2048]{1,0:T(8,128)(2,1)S(1)} %get-tuple-element.54.refs_0_), channel_id=1, source_target_pairs={{0,3},{1,0},{2,1},{3,2},{4,7},{5,4},{6,5},{7,6},{8,11},{9,8},{10,9... | collective-permute-start | bytes 1179656 | tf_op jit(solution)/shard_map/ppermute | solution.py:630
  71.7 20.5 %collective-permute-start.12 = (bf16[96,2048]{1,0:T(8,128)(2,1)S(1)}, bf16[96,2048]{1,0:T(8,128)(2,1)S(1)}, u32[]{:S(2)}, u32[]{:S(2)}) collective-permute-start(bf16[96,2048]{1,0:T(8,128)(2,1)S(1)} %get-tuple-element.54.refs_0_), channel_id=1, source_target_pairs={{0,1},{1,2},{2,3},{3,0},{4,5},{5,6},{6,7},{7,4},{8,9},{9,10},{10,1... | collective-permute-start | bytes 1179656 | tf_op jit(solution)/shard_map/ppermute | solution.py:629
  71.7 20.5 %collective-permute-start.11 = (bf16[96,2048]{1,0:T(8,128)(2,1)S(1)}, bf16[96,2048]{1,0:T(8,128)(2,1)S(1)}, u32[]{:S(2)}, u32[]{:S(2)}) collective-permute-start(bf16[96,2048]{1,0:T(8,128)(2,1)S(1)} %get-tuple-element.54.refs_0_), channel_id=1, source_target_pairs={{0,2},{1,3},{2,0},{3,1},{4,6},{5,7},{6,4},{7,5},{8,10},{9,11},{10,... | collective-permute-start | bytes 1179656 | tf_op jit(solution)/shard_map/ppermute | solution.py:628
  101.5 6.5 %collective-permute-start.15 = (bf16[48,2048]{1,0:T(8,128)(2,1)S(1)}, bf16[48,2048]{1,0:T(8,128)(2,1)S(1)}, u32[]{:S(2)}, u32[]{:S(2)}) collective-permute-start(bf16[48,2048]{1,0:T(8,128)(2,1)S(1)} %get-tuple-element.61), channel_id=1, source_target_pairs={{0,3},{1,0},{2,1},{3,2},{4,7},{5,4},{6,5},{7,6},{8,11},{9,8},{10,9... | collective-permute-start | bytes 589832 | tf_op jit(solution)/shard_map/ppermute | solution.py:633
  101.9 7.0 %collective-permute-start.16 = (bf16[48,2048]{1,0:T(8,128)(2,1)S(1)}, bf16[48,2048]{1,0:T(8,128)(2,1)S(1)}, u32[]{:S(2)}, u32[]{:S(2)}) collective-permute-start(bf16[48,2048]{1,0:T(8,128)(2,1)S(1)} %get-tuple-element.63), channel_id=1, source_target_pairs={{0,1},{1,2},{2,3},{3,0},{4,5},{5,6},{6,7},{7,4},{8,9},{9,10},{10,1... | collective-permute-start | bytes 589832 | tf_op jit(solution)/shard_map/ppermute | solution.py:632
  105.6 10.7 %collective-permute-start.14 = (bf16[48,2048]{1,0:T(8,128)(2,1)S(1)}, bf16[48,2048]{1,0:T(8,128)(2,1)S(1)}, u32[]{:S(2)}, u32[]{:S(2)}) collective-permute-start(bf16[48,2048]{1,0:T(8,128)(2,1)S(1)} %get-tuple-element.59), channel_id=1, source_target_pairs={{0,3},{1,0},{2,1},{3,2},{4,7},{5,4},{6,5},{7,6},{8,11},{9,8},{10,9... | collective-permute-start | bytes 589832 | tf_op jit(solution)/shard_map/ppermute | solution.py:635
  107.2 9.1 %collective-permute-start.19 = (bf16[48,2048]{1,0:T(8,128)(2,1)S(1)}, bf16[48,2048]{1,0:T(8,128)(2,1)S(1)}, u32[]{:S(2)}, u32[]{:S(2)}) collective-permute-start(bf16[48,2048]{1,0:T(8,128)(2,1)S(1)} %get-tuple-element.66), channel_id=1, source_target_pairs={{0,1},{1,2},{2,3},{3,0},{4,5},{5,6},{6,7},{7,4},{8,9},{9,10},{10,1... | collective-permute-start | bytes 589832 | tf_op jit(solution)/shard_map/ppermute | solution.py:636
  109.0 8.9 %collective-permute-start.17 = (bf16[48,2048]{1,0:T(8,128)(2,1)S(1)}, bf16[48,2048]{1,0:T(8,128)(2,1)S(1)}, u32[]{:S(2)}, u32[]{:S(2)}) collective-permute-start(bf16[48,2048]{1,0:T(8,128)(2,1)S(1)} %get-tuple-element.64), channel_id=1, source_target_pairs={{0,1},{1,2},{2,3},{3,0},{4,5},{5,6},{6,7},{7,4},{8,9},{9,10},{10,1... | collective-permute-start | bytes 589832 | tf_op jit(solution)/shard_map/ppermute | solution.py:639
  110.1 7.8 %collective-permute-start.18 = (bf16[48,2048]{1,0:T(8,128)(2,1)S(1)}, bf16[48,2048]{1,0:T(8,128)(2,1)S(1)}, u32[]{:S(2)}, u32[]{:S(2)}) collective-permute-start(bf16[48,2048]{1,0:T(8,128)(2,1)S(1)} %get-tuple-element.65), channel_id=1, source_target_pairs={{0,3},{1,0},{2,1},{3,2},{4,7},{5,4},{6,5},{7,6},{8,11},{9,8},{10,9... | collective-permute-start | bytes 589832 | tf_op jit(solution)/shard_map/ppermute | solution.py:638
Sparse Core Ops, SparseCore 0:
  9.6 79.2 all-gather.1
where the time goes:
time: 126 us
  waiting for transfers between devices  46.5 us (37%)
  Pallas kernels  34.8 us (28%)
  starting transfers between devices  28.8 us (23%)
  between operations  13.6 us (11%)
  other arithmetic  2 us (2%)
    pallas_call x13, Pallas kernels, call(): pl.pallas_call(kernel, in_specs=[FAR] * len(far) + [FULL] * len(near), ou...  33.9 us
    ppermute x3, waiting for transfers between devices, per_device(): lax.ppermute(parts[k], 'tp', ring(size, k))  16.1 us
    ppermute x1, waiting for transfers between devices, per_device(): left = lax.ppermute(normed, 'tp', ring(size, -1))  14.7 us
    ppermute x3, starting transfers between devices, per_device(): lax.ppermute(parts[k], 'tp', ring(size, k))  5.72 us
    ppermute x3, starting transfers between devices, state_ahead(): planes = [lax.ppermute(whole, plane, ring(size, k)) for k in range(1, size)]  5.64 us
    ppermute x3, starting transfers between devices, state_ahead(): lax.ppermute(chip, line, ring(size, k))  4.79 us
    ppermute x3, waiting for transfers between devices, state_ahead(): lax.ppermute(chip, line, ring(size, k))  3.8 us
    ppermute x1, waiting for transfers between devices, per_device(): right = lax.ppermute(normed, 'tp', ring(size, 1))  3.41 us
  transfers between devices with their start and end apart: 21, of which 13 were waited for; matrix products, arithmetic and copies ran while one was open for 0% of the time, Pallas kernels for 20%

commit v1 on v0

--- a/solution.py
+++ b/solution.py
@@ -34,6 +34,10 @@
         scratch_shapes=scratch,
         compiler_params=pltpu.CompilerParams(vmem_limit_bytes=mib << 20),
     )(*far, *near)
+
+
+def upward(size, k):
+    return [(i, i + k) for i in range(size - k)]
 
 
 def ring(size, k):
@@ -362,7 +366,7 @@
         row_kernel, lines, [(half, BF), (half, BF)], [pltpu.VMEM((size, *half), BF)], far=[early[1]]
     )
     size = lax.axis_size(plane)
-    planes = [lax.ppermute(whole, plane, ring(size, k)) for k in range(1, size)]
+    planes = [lax.ppermute(whole, plane, upward(size, k)) for k in range(1, size)]
     late = then(whole)
     (state,) = call(plane_kernel, [before] + planes, [(half, BF)], far=[late[1]])
     return early, late, (other, state, lax.ppermute(state, core, swap))
@@ -446,7 +450,7 @@
 TILE = 128
 STRIP = 256
 AHEAD = 3
-UP_GROUPS = (3, 5, 3)
+UP_GROUPS = (5, 6)
 DOWN_GROUPS = (5, 3)
 
 

time: 126 us -> 127 us (level)
  starting transfers between devices: 28.8 us -> 33.4 us
  waiting for transfers between devices: 46.5 us -> 43.2 us
    ppermute x3, starting transfers between devices: 5.64 us -> 10.5 us  [state_ahead(): lax.ppermute(whole, plane, upward(size, k))]
    ppermute x3, waiting for transfers between devices: 3.4 us -> 0.01 us  [state_ahead(): lax.ppermute(whole, plane, upward(size, k))]
  transfers between devices with their start and end apart: 21 -> 21, of which waited for: 13 -> 11; matrix products, arithmetic and copies ran while one was open for 0% -> 0% of each run, Pallas kernels for 20% -> 19%
where the time goes in v1:
time: 127 us
  waiting for transfers between devices  43.2 us (34%)
  Pallas kernels  34.5 us (27%)
  starting transfers between devices  33.4 us (26%)
  between operations  13.6 us (11%)
  other arithmetic  2 us (2%)
    pallas_call x13, Pallas kernels, call(): pl.pallas_call(kernel, in_specs=[FAR] * len(far) + [FULL] * len(near), ou...  33.5 us
    ppermute x3, waiting for transfers between devices, per_device(): lax.ppermute(parts[k], 'tp', ring(size, k))  16.1 us
    ppermute x1, waiting for transfers between devices, per_device(): left = lax.ppermute(normed, 'tp', ring(size, -1))  14.7 us
    ppermute x3, starting transfers between devices, state_ahead(): lax.ppermute(whole, plane, upward(size, k))  10.5 us
    ppermute x3, starting transfers between devices, per_device(): lax.ppermute(parts[k], 'tp', ring(size, k))  5.72 us
    ppermute x3, starting transfers between devices, state_ahead(): lax.ppermute(chip, line, ring(size, k))  4.79 us
    ppermute x3, waiting for transfers between devices, state_ahead(): lax.ppermute(chip, line, ring(size, k))  3.8 us
    ppermute x1, waiting for transfers between devices, per_device(): right = lax.ppermute(normed, 'tp', ring(size, 1))  3.41 us
  transfers between devices with their start and end apart: 21, of which 11 were waited for; matrix products, arithmetic and copies ran while one was open for 0% of the time, Pallas kernels for 19%

profile of v1, /device:TPU:0, one launch (start us, length us, event | category | flops | bytes accessed | tf_op | source)
XLA Modules:
  0.0 126.7 jit_solution(342224758904283322)
XLA Ops:
  6.5 2.0 %pad_maximum_fusion = bf16[64,4224]{1,0:T(8,128)(2,1)} fusion(bf16[64,1408]{1,0:T(8,128)(2,1)} %bitcast.5, bf16[64,1408]{1,0:T(8,128)(2,1)} %param.24, bf16[64,1408]{1,0:T(8,128)(2,1)} %param.23), kind=kLoop, calls=%fused_computation | loop fusion | flops 1622016 | bytes 1081344 | tf_op jit(solution)/shard_map/concatenate | solution.py:618
  8.5 0.0 all-gather.2.cloned.1.call-update
  8.6 8.1 %shard_map.127 = (bf16[12,128,128]{2,1,0:T(8,128)(2,1)S(1)}, bf16[4,128,128]{2,1,0:T(8,128)(2,1)S(1)}, bf16[12,128,384]{2,1,0:T(8,128)(2,1)S(1)}, bf16[12,128,256]{2,1,0:T(8,128)(2,1)S(1)}, f32[384,512]{1,0:T(8,128)S(1)}) custom-call(bf16[384,512]{1,0:T(8,128)(2,1)} %k_far_ref.1, bf16[384,512]{1,0:T(8,128)(2,1)} %v_far_ref.1, f32[8,384]{1,0:T(8,128)} %beta_far_ref.1, ...), custom_call_target="tpu_custom_call" | custom-call | tf_op jit(solution)/shard_map/pallas_call | solution.py:29
  16.6 0.1 collective-permute-start
  16.7 1.3 %collective-permute-done.other_ref = bf16[4,128,128]{2,1,0:T(8,128)(2,1)S(1)} collective-permute-done((bf16[4,128,128]{2,1,0:T(8,128)(2,1)S(1)}, bf16[4,128,128]{2,1,0:T(8,128)(2,1)S(1)}, u32[]{:S(2)}, u32[]{:S(2)}) %collective-permute-start) | collective-permute-done | bytes 131104 | tf_op jit(solution)/shard_map/ppermute | solution.py:360
  18.1 0.2 shard_map.128
  18.3 3.2 %collective-permute-start.3 = (bf16[2,128,128]{2,1,0:T(8,128)(2,1)S(1)}, bf16[2,128,128]{2,1,0:T(8,128)(2,1)S(1)}, u32[]{:S(2)}, u32[]{:S(2)}) collective-permute-start(bf16[2,128,128]{2,1,0:T(8,128)(2,1)S(1)} %get-tuple-element.37.after_ref.rest_0_), channel_id=1, source_target_pairs={{0,24},{8,0},{16,8},{24,16},{1,25},{9,1},{17,9},{25,17},{2,26},{10... | collective-permute-start | bytes 196616 | tf_op jit(solution)/shard_map/ppermute | solution.py:363
  21.5 0.6 collective-permute-start.2
  22.1 1.0 collective-permute-start.1
  23.1 2.9 %shard_map.129 = (f32[384,256]{1,0:T(8,128)S(1)}, bf16[384,256]{1,0:T(8,128)(2,1)S(1)}) custom-call(bf16[2,128,128]{2,1,0:T(8,128)(2,1)S(1)} %get-tuple-element.37.after_ref.rest_0_, bf16[384,512]{1,0:T(8,128)(2,1)S(1)} %copy-done.1, bf16[12,128,256]{2,1,0:T(8,128)(2,1)S(1)} %get-tuple-element.38.d_ref, bf16[12,128,384]{2,1,0:T(8,128)(2,1)S(1)} %get-tuple-element.39.y_ref, ...), custom_call_target="tpu_custom_call" | custom-call | tf_op jit(solution)/shard_map/pallas_call | solution.py:29
  26.0 2.9 %collective-permute-done.2.rest_2_ = bf16[2,128,128]{2,1,0:T(8,128)(2,1)S(1)} collective-permute-done((bf16[2,128,128]{2,1,0:T(8,128)(2,1)S(1)}, bf16[2,128,128]{2,1,0:T(8,128)(2,1)S(1)}, u32[]{:S(2)}, u32[]{:S(2)}) %collective-permute-start.2) | collective-permute-done | bytes 65568 | tf_op jit(solution)/shard_map/ppermute | solution.py:363
  28.9 0.9 collective-permute-done.1.rest_1_
  29.8 0.6 shard_map.130
  30.5 0.0 copy-start.3
  30.5 0.0 copy-start.5
  30.5 6.4 %collective-permute-start.6 = (bf16[2,128,128]{2,1,0:T(8,128)(2,1)S(1)}, bf16[2,128,128]{2,1,0:T(8,128)(2,1)S(1)}, u32[]{:S(2)}, u32[]{:S(2)}) collective-permute-start(bf16[2,128,128]{2,1,0:T(8,128)(2,1)S(1)} %get-tuple-element.44.after_ref), channel_id=1, source_target_pairs={{0,96},{1,97},{2,98},{3,99},{4,100},{5,101},{6,102},{7,103},{8,104... | collective-permute-start | bytes 196616 | tf_op jit(solution)/shard_map/ppermute | solution.py:369
  36.9 1.3 %collective-permute-start.5 = (bf16[2,128,128]{2,1,0:T(8,128)(2,1)S(1)}, bf16[2,128,128]{2,1,0:T(8,128)(2,1)S(1)}, u32[]{:S(2)}, u32[]{:S(2)}) collective-permute-start(bf16[2,128,128]{2,1,0:T(8,128)(2,1)S(1)} %get-tuple-element.44.after_ref), channel_id=1, source_target_pairs={{0,64},{32,96},{1,65},{33,97},{2,66},{34,98},{3,67},{35,99},{4,68}... | collective-permute-start | bytes 196616 | tf_op jit(solution)/shard_map/ppermute | solution.py:369
  38.2 2.8 %collective-permute-start.4 = (bf16[2,128,128]{2,1,0:T(8,128)(2,1)S(1)}, bf16[2,128,128]{2,1,0:T(8,128)(2,1)S(1)}, u32[]{:S(2)}, u32[]{:S(2)}) collective-permute-start(bf16[2,128,128]{2,1,0:T(8,128)(2,1)S(1)} %get-tuple-element.44.after_ref), channel_id=1, source_target_pairs={{0,32},{32,64},{64,96},{1,33},{33,65},{65,97},{2,34},{34,66},{66,9... | collective-permute-start | bytes 196616 | tf_op jit(solution)/shard_map/ppermute | solution.py:369
  41.0 2.9 %shard_map.131 = (f32[384,256]{1,0:T(8,128)S(1)}, bf16[384,256]{1,0:T(8,128)(2,1)S(1)}) custom-call(bf16[2,128,128]{2,1,0:T(8,128)(2,1)S(1)} %get-tuple-element.44.after_ref, bf16[384,512]{1,0:T(8,128)(2,1)S(1)} %copy-done.1, bf16[12,128,256]{2,1,0:T(8,128)(2,1)S(1)} %get-tuple-element.38.d_ref, bf16[12,128,384]{2,1,0:T(8,128)(2,1)S(1)} %get-tuple-element.39.y_ref, ...), custom_call_target="tpu_custom_call" | custom-call | tf_op jit(solution)/shard_map/pallas_call | solution.py:29
  44.0 0.9 shard_map.132.mine_ref
  44.9 0.1 collective-permute-start.7
  45.0 0.3 shard_map.133.gate_ref
  45.3 0.9 collective-permute-done.7.theirs_ref
  46.2 2.1 %shard_map.134 = (f32[96,2048]{1,0:T(8,128)S(1)}, bf16[96,2048]{1,0:T(8,128)(2,1)S(1)}, bf16[96,2048]{1,0:T(8,128)(2,1)S(1)}, bf16[96,2048]{1,0:T(8,128)(2,1)S(1)}) custom-call(f32[384,256]{1,0:T(8,128)S(1)} %get-tuple-element.42.o0_ref, bf16[384,256]{1,0:T(8,128)(2,1)S(1)} %get-tuple-element.43.after_ref.q0_ref, f32[384,256]{1,0:T(8,128)S(1)} %get-tuple-element.45.o1_ref, ...), custom_call_target="tpu_custom_call" | custom-call | tf_op jit(solution)/shard_map/pallas_call | solution.py:29
  48.4 1.6 %collective-permute-start.8 = (bf16[96,2048]{1,0:T(8,128)(2,1)S(1)}, bf16[96,2048]{1,0:T(8,128)(2,1)S(1)}, u32[]{:S(2)}, u32[]{:S(2)}) collective-permute-start(bf16[96,2048]{1,0:T(8,128)(2,1)S(1)} %get-tuple-element.50), channel_id=1, source_target_pairs={{0,1},{1,2},{2,3},{3,0},{4,5},{5,6},{6,7},{7,4},{8,9},{9,10},{10,1... | collective-permute-start | bytes 1179656 | tf_op jit(solution)/shard_map/ppermute | solution.py:630
  49.9 2.7 %collective-permute-start.9 = (bf16[96,2048]{1,0:T(8,128)(2,1)S(1)}, bf16[96,2048]{1,0:T(8,128)(2,1)S(1)}, u32[]{:S(2)}, u32[]{:S(2)}) collective-permute-start(bf16[96,2048]{1,0:T(8,128)(2,1)S(1)} %get-tuple-element.51), channel_id=1, source_target_pairs={{0,2},{1,3},{2,0},{3,1},{4,6},{5,7},{6,4},{7,5},{8,10},{9,11},{10,... | collective-permute-start | bytes 1179656 | tf_op jit(solution)/shard_map/ppermute | solution.py:630
  52.6 1.4 %collective-permute-start.10 = (bf16[96,2048]{1,0:T(8,128)(2,1)S(1)}, bf16[96,2048]{1,0:T(8,128)(2,1)S(1)}, u32[]{:S(2)}, u32[]{:S(2)}) collective-permute-start(bf16[96,2048]{1,0:T(8,128)(2,1)S(1)} %get-tuple-element.52), channel_id=1, source_target_pairs={{0,3},{1,0},{2,1},{3,2},{4,7},{5,4},{6,5},{7,6},{8,11},{9,8},{10,9... | collective-permute-start | bytes 1179656 | tf_op jit(solution)/shard_map/ppermute | solution.py:630
  54.1 6.7 %collective-permute-done.8.rest_1_ = bf16[96,2048]{1,0:T(8,128)(2,1)S(1)} collective-permute-done((bf16[96,2048]{1,0:T(8,128)(2,1)S(1)}, bf16[96,2048]{1,0:T(8,128)(2,1)S(1)}, u32[]{:S(2)}, u32[]{:S(2)}) %collective-permute-start.8) | collective-permute-done | bytes 393248 | tf_op jit(solution)/shard_map/ppermute | solution.py:630
  60.8 9.4 %collective-permute-done.9.rest_2_ = bf16[96,2048]{1,0:T(8,128)(2,1)S(1)} collective-permute-done((bf16[96,2048]{1,0:T(8,128)(2,1)S(1)}, bf16[96,2048]{1,0:T(8,128)(2,1)S(1)}, u32[]{:S(2)}, u32[]{:S(2)}) %collective-permute-start.9) | collective-permute-done | bytes 393248 | tf_op jit(solution)/shard_map/ppermute | solution.py:630
  70.2 0.4 shard_map.135
  70.7 2.4 %collective-permute-start.13 = (bf16[96,2048]{1,0:T(8,128)(2,1)S(1)}, bf16[96,2048]{1,0:T(8,128)(2,1)S(1)}, u32[]{:S(2)}, u32[]{:S(2)}) collective-permute-start(bf16[96,2048]{1,0:T(8,128)(2,1)S(1)} %get-tuple-element.54.refs_0_), channel_id=1, source_target_pairs={{0,3},{1,0},{2,1},{3,2},{4,7},{5,4},{6,5},{7,6},{8,11},{9,8},{10,9... | collective-permute-start | bytes 1179656 | tf_op jit(solution)/shard_map/ppermute | solution.py:634
  73.1 2.3 %collective-permute-start.11 = (bf16[96,2048]{1,0:T(8,128)(2,1)S(1)}, bf16[96,2048]{1,0:T(8,128)(2,1)S(1)}, u32[]{:S(2)}, u32[]{:S(2)}) collective-permute-start(bf16[96,2048]{1,0:T(8,128)(2,1)S(1)} %get-tuple-element.54.refs_0_), channel_id=1, source_target_pairs={{0,2},{1,3},{2,0},{3,1},{4,6},{5,7},{6,4},{7,5},{8,10},{9,11},{10,... | collective-permute-start | bytes 1179656 | tf_op jit(solution)/shard_map/ppermute | solution.py:632
  75.4 14.7 %collective-permute-done.13.left_ref = bf16[96,2048]{1,0:T(8,128)(2,1)S(1)} collective-permute-done((bf16[96,2048]{1,0:T(8,128)(2,1)S(1)}, bf16[96,2048]{1,0:T(8,128)(2,1)S(1)}, u32[]{:S(2)}, u32[]{:S(2)}) %collective-permute-start.13) | collective-permute-done | bytes 393248 | tf_op jit(solution)/shard_map/ppermute | solution.py:634
  90.2 3.4 %collective-permute-done.12.right_ref = bf16[96,2048]{1,0:T(8,128)(2,1)S(1)} collective-permute-done((bf16[96,2048]{1,0:T(8,128)(2,1)S(1)}, bf16[96,2048]{1,0:T(8,128)(2,1)S(1)}, u32[]{:S(2)}, u32[]{:S(2)}) %collective-permute-start.12) | collective-permute-done | bytes 393248 | tf_op jit(solution)/shard_map/ppermute | solution.py:633
  93.6 8.9 %shard_map.136 = (bf16[48,2048]{1,0:T(8,128)(2,1)S(1)}, bf16[48,2048]{1,0:T(8,128)(2,1)S(1)}, bf16[192,1408]{1,0:T(8,128)(2,1)S(1)}, bf16[2048,1408]{1,0:T(8,128...) custom-call(bf16[2048,4224]{1,0:T(8,128)(2,1)} %all-gather.2.cloned.1.call-done.w_ref, ...), custom_call_target="tpu_custom_call" | custom-call | tf_op jit(solution)/shard_map/pallas_call | solution.py:29
  102.5 0.4 collective-permute-start.15
  102.9 1.7 %collective-permute-start.16 = (bf16[48,2048]{1,0:T(8,128)(2,1)S(1)}, bf16[48,2048]{1,0:T(8,128)(2,1)S(1)}, u32[]{:S(2)}, u32[]{:S(2)}) collective-permute-start(bf16[48,2048]{1,0:T(8,128)(2,1)S(1)} %get-tuple-element.63), channel_id=1, source_target_pairs={{0,1},{1,2},{2,3},{3,0},{4,5},{5,6},{6,7},{7,4},{8,9},{9,10},{10,1... | collective-permute-start | bytes 589832 | tf_op jit(solution)/shard_map/ppermute | solution.py:636
  104.6 2.0 %shard_map.138 = (bf16[48,2048]{1,0:T(8,128)(2,1)S(1)}, bf16[48,2048]{1,0:T(8,128)(2,1)S(1)}, bf16[48,2048]{1,0:T(8,128)(2,1)S(1)}, bf16[48,2048]{1,0:T(8,128)(2,1)S(1)}) custom-call(bf16[192,1408]{1,0:T(8,128)(2,1)S(1)} %get-tuple-element.58.hidden_ref, bf16[2048,1408]{1,0:T(8,128)(2,1)S(1)} %get-tuple-element.57.refs_3_.down_ref), custom_call_target="tpu_custom_call" | custom-call | tf_op jit(solution)/shard_map/pallas_call | solution.py:29
  106.7 1.6 %collective-permute-start.14 = (bf16[48,2048]{1,0:T(8,128)(2,1)S(1)}, bf16[48,2048]{1,0:T(8,128)(2,1)S(1)}, u32[]{:S(2)}, u32[]{:S(2)}) collective-permute-start(bf16[48,2048]{1,0:T(8,128)(2,1)S(1)} %get-tuple-element.59), channel_id=1, source_target_pairs={{0,3},{1,0},{2,1},{3,2},{4,7},{5,4},{6,5},{7,6},{8,11},{9,8},{10,9... | collective-permute-start | bytes 589832 | tf_op jit(solution)/shard_map/ppermute | solution.py:639
  108.3 0.5 collective-permute-start.19
  108.8 0.2 collective-permute-done.15.more_low_ref
  109.0 0.9 collective-permute-done.16.more_high_ref
  109.9 0.1 shard_map.139
  110.0 1.2 collective-permute-start.17
  111.2 2.1 %collective-permute-start.18 = (bf16[48,2048]{1,0:T(8,128)(2,1)S(1)}, bf16[48,2048]{1,0:T(8,128)(2,1)S(1)}, u32[]{:S(2)}, u32[]{:S(2)}) collective-permute-start(bf16[48,2048]{1,0:T(8,128)(2,1)S(1)} %get-tuple-element.65), channel_id=1, source_target_pairs={{0,3},{1,0},{2,1},{3,2},{4,7},{5,4},{6,5},{7,6},{8,11},{9,8},{10,9... | collective-permute-start | bytes 589832 | tf_op jit(solution)/shard_map/ppermute | solution.py:642
  113.3 4.0 %shard_map.137.own_ref = bf16[96,2048]{1,0:T(8,128)(2,1)S(1)} custom-call(bf16[96,2048]{1,0:T(8,128)(2,1)S(1)} %get-tuple-element.54.refs_0_, bf16[2048,1408]{1,0:T(8,128)(2,1)S(1)} %get-tuple-element.55.refs_1_, bf16[2048,1408]{1,0:T(8,128)(2,1)S(1)} %get-tuple-element.56.refs_2_, bf16[2048,1408]{1,0:T(8,128)(2,1)S(1)} %get-tuple-element.57.refs_3_.down_ref), custom_call_target="tpu_custom_call" | custom-call | tf_op jit(solution)/shard_map/pallas_call | solution.py:29
  117.3 1.6 %collective-permute-done.17.rest_1_ = bf16[48,2048]{1,0:T(8,128)(2,1)S(1)} collective-permute-done((bf16[48,2048]{1,0:T(8,128)(2,1)S(1)}, bf16[48,2048]{1,0:T(8,128)(2,1)S(1)}, u32[]{:S(2)}, u32[]{:S(2)}) %collective-permute-start.17) | collective-permute-done | bytes 196640 | tf_op jit(solution)/shard_map/ppermute | solution.py:643
  118.9 1.0 last_sum.1
  (22 shorter events, 0.1 us)
Async XLA Ops:
  6.5 87.0 %all-gather.2.cloned.1.call-start = ((), (), s32[]{:S(2)}) async-start(), calls=%async_computation | async-start | bytes 17842176 | tf_op jit(solution)/shard_map/all_gather | solution.py:619
  6.5 16.5 %copy-start.1 = (bf16[384,512]{1,0:T(8,128)(2,1)S(1)}, bf16[384,512]{1,0:T(8,128)(2,1)}, u32[]{:S(2)}) copy-start(bf16[384,512]{1,0:T(8,128)(2,1)} %q_ref.3) | copy-start | bytes 1179652
  16.6 1.4 %collective-permute-start = (bf16[4,128,128]{2,1,0:T(8,128)(2,1)S(1)}, bf16[4,128,128]{2,1,0:T(8,128)(2,1)S(1)}, u32[]{:S(2)}, u32[]{:S(2)}) collective-permute-start(bf16[4,128,128]{2,1,0:T(8,128)(2,1)S(1)} %get-tuple-element.36.own_ref), channel_id=1, source_target_pairs={{0,4},{4,0},{1,5},{5,1},{2,6},{6,2},{3,7},{7,3},{8,12},{12,8},{9,1... | collective-permute-start | bytes 393224 | tf_op jit(solution)/shard_map/ppermute | solution.py:360
  18.3 7.7 %collective-permute-start.3 = (bf16[2,128,128]{2,1,0:T(8,128)(2,1)S(1)}, bf16[2,128,128]{2,1,0:T(8,128)(2,1)S(1)}, u32[]{:S(2)}, u32[]{:S(2)}) collective-permute-start(bf16[2,128,128]{2,1,0:T(8,128)(2,1)S(1)} %get-tuple-element.37.after_ref.rest_0_), channel_id=1, source_target_pairs={{0,24},{8,0},{16,8},{24,16},{1,25},{9,1},{17,9},{25,17},{2,26},{10... | collective-permute-start | bytes 196616 | tf_op jit(solution)/shard_map/ppermute | solution.py:363
  21.5 7.4 %collective-permute-start.2 = (bf16[2,128,128]{2,1,0:T(8,128)(2,1)S(1)}, bf16[2,128,128]{2,1,0:T(8,128)(2,1)S(1)}, u32[]{:S(2)}, u32[]{:S(2)}) collective-permute-start(bf16[2,128,128]{2,1,0:T(8,128)(2,1)S(1)} %get-tuple-element.37.after_ref.rest_0_), channel_id=1, source_target_pairs={{0,16},{8,24},{16,0},{24,8},{1,17},{9,25},{17,1},{25,9},{2,18},{10... | collective-permute-start | bytes 196616 | tf_op jit(solution)/shard_map/ppermute | solution.py:363
  22.1 7.7 %collective-permute-start.1 = (bf16[2,128,128]{2,1,0:T(8,128)(2,1)S(1)}, bf16[2,128,128]{2,1,0:T(8,128)(2,1)S(1)}, u32[]{:S(2)}, u32[]{:S(2)}) collective-permute-start(bf16[2,128,128]{2,1,0:T(8,128)(2,1)S(1)} %get-tuple-element.37.after_ref.rest_0_), channel_id=1, source_target_pairs={{0,8},{8,16},{16,24},{24,0},{1,9},{9,17},{17,25},{25,1},{2,10},{10... | collective-permute-start | bytes 196616 | tf_op jit(solution)/shard_map/ppermute | solution.py:363
  30.5 14.5 %copy-start.3 = (bf16[384,512]{1,0:T(8,128)(2,1)S(1)}, bf16[384,512]{1,0:T(8,128)(2,1)}, u32[]{:S(2)}) copy-start(bf16[384,512]{1,0:T(8,128)(2,1)} %gates_ref.1) | copy-start | bytes 1179652
  30.5 14.5 %copy-start.5 = (f32[64]{0:T(128)S(1)}, f32[64]{0:T(128)}, u32[]{:S(2)}) copy-start(f32[64]{0:T(128)} %param.19) | copy-start | bytes 772
  30.5 13.5 %collective-permute-start.6 = (bf16[2,128,128]{2,1,0:T(8,128)(2,1)S(1)}, bf16[2,128,128]{2,1,0:T(8,128)(2,1)S(1)}, u32[]{:S(2)}, u32[]{:S(2)}) collective-permute-start(bf16[2,128,128]{2,1,0:T(8,128)(2,1)S(1)} %get-tuple-element.44.after_ref), channel_id=1, source_target_pairs={{0,96},{1,97},{2,98},{3,99},{4,100},{5,101},{6,102},{7,103},{8,104... | collective-permute-start | bytes 196616 | tf_op jit(solution)/shard_map/ppermute | solution.py:369
  36.9 7.0 %collective-permute-start.5 = (bf16[2,128,128]{2,1,0:T(8,128)(2,1)S(1)}, bf16[2,128,128]{2,1,0:T(8,128)(2,1)S(1)}, u32[]{:S(2)}, u32[]{:S(2)}) collective-permute-start(bf16[2,128,128]{2,1,0:T(8,128)(2,1)S(1)} %get-tuple-element.44.after_ref), channel_id=1, source_target_pairs={{0,64},{32,96},{1,65},{33,97},{2,66},{34,98},{3,67},{35,99},{4,68}... | collective-permute-start | bytes 196616 | tf_op jit(solution)/shard_map/ppermute | solution.py:369
  38.2 5.7 %collective-permute-start.4 = (bf16[2,128,128]{2,1,0:T(8,128)(2,1)S(1)}, bf16[2,128,128]{2,1,0:T(8,128)(2,1)S(1)}, u32[]{:S(2)}, u32[]{:S(2)}) collective-permute-start(bf16[2,128,128]{2,1,0:T(8,128)(2,1)S(1)} %get-tuple-element.44.after_ref), channel_id=1, source_target_pairs={{0,32},{32,64},{64,96},{1,33},{33,65},{65,97},{2,34},{34,66},{66,9... | collective-permute-start | bytes 196616 | tf_op jit(solution)/shard_map/ppermute | solution.py:369
  41.0 5.2 %copy-start = (bf16[512,2048]{1,0:T(8,128)(2,1)S(1)}, bf16[512,2048]{1,0:T(8,128)(2,1)}, u32[]{:S(2)}) copy-start(bf16[512,2048]{1,0:T(8,128)(2,1)} %w_ref.1) | copy-start | bytes 6291460
  44.9 1.3 %collective-permute-start.7 = (bf16[2,128,128]{2,1,0:T(8,128)(2,1)S(1)}, bf16[2,128,128]{2,1,0:T(8,128)(2,1)S(1)}, u32[]{:S(2)}, u32[]{:S(2)}) collective-permute-start(bf16[2,128,128]{2,1,0:T(8,128)(2,1)S(1)} %shard_map.132.mine_ref), channel_id=1, source_target_pairs={{0,4},{4,0},{1,5},{5,1},{2,6},{6,2},{3,7},{7,3},{8,12},{12,8},{9,1... | collective-permute-start | bytes 196616 | tf_op jit(solution)/shard_map/ppermute | solution.py:372
  46.2 24.0 %copy-start.2 = (bf16[96,2048]{1,0:T(8,128)(2,1)S(1)}, bf16[96,2048]{1,0:T(8,128)(2,1)}, u32[]{:S(2)}) copy-start(bf16[96,2048]{1,0:T(8,128)(2,1)} %stream_ref.1) | copy-start | bytes 1179652
  46.2 24.0 %copy-start.4 = (f32[2048]{0:T(1024)S(1)}, f32[2048]{0:T(1024)}, u32[]{:S(2)}) copy-start(f32[2048]{0:T(1024)} %param.22) | copy-start | bytes 24580
  48.4 12.5 %collective-permute-start.8 = (bf16[96,2048]{1,0:T(8,128)(2,1)S(1)}, bf16[96,2048]{1,0:T(8,128)(2,1)S(1)}, u32[]{:S(2)}, u32[]{:S(2)}) collective-permute-start(bf16[96,2048]{1,0:T(8,128)(2,1)S(1)} %get-tuple-element.50), channel_id=1, source_target_pairs={{0,1},{1,2},{2,3},{3,0},{4,5},{5,6},{6,7},{7,4},{8,9},{9,10},{10,1... | collective-permute-start | bytes 1179656 | tf_op jit(solution)/shard_map/ppermute | solution.py:630
  49.9 20.3 %collective-permute-start.9 = (bf16[96,2048]{1,0:T(8,128)(2,1)S(1)}, bf16[96,2048]{1,0:T(8,128)(2,1)S(1)}, u32[]{:S(2)}, u32[]{:S(2)}) collective-permute-start(bf16[96,2048]{1,0:T(8,128)(2,1)S(1)} %get-tuple-element.51), channel_id=1, source_target_pairs={{0,2},{1,3},{2,0},{3,1},{4,6},{5,7},{6,4},{7,5},{8,10},{9,11},{10,... | collective-permute-start | bytes 1179656 | tf_op jit(solution)/shard_map/ppermute | solution.py:630
  52.6 17.6 %collective-permute-start.10 = (bf16[96,2048]{1,0:T(8,128)(2,1)S(1)}, bf16[96,2048]{1,0:T(8,128)(2,1)S(1)}, u32[]{:S(2)}, u32[]{:S(2)}) collective-permute-start(bf16[96,2048]{1,0:T(8,128)(2,1)S(1)} %get-tuple-element.52), channel_id=1, source_target_pairs={{0,3},{1,0},{2,1},{3,2},{4,7},{5,4},{6,5},{7,6},{8,11},{9,8},{10,9... | collective-permute-start | bytes 1179656 | tf_op jit(solution)/shard_map/ppermute | solution.py:630
  70.7 19.5 %collective-permute-start.13 = (bf16[96,2048]{1,0:T(8,128)(2,1)S(1)}, bf16[96,2048]{1,0:T(8,128)(2,1)S(1)}, u32[]{:S(2)}, u32[]{:S(2)}) collective-permute-start(bf16[96,2048]{1,0:T(8,128)(2,1)S(1)} %get-tuple-element.54.refs_0_), channel_id=1, source_target_pairs={{0,3},{1,0},{2,1},{3,2},{4,7},{5,4},{6,5},{7,6},{8,11},{9,8},{10,9... | collective-permute-start | bytes 1179656 | tf_op jit(solution)/shard_map/ppermute | solution.py:634
  73.1 20.5 %collective-permute-start.12 = (bf16[96,2048]{1,0:T(8,128)(2,1)S(1)}, bf16[96,2048]{1,0:T(8,128)(2,1)S(1)}, u32[]{:S(2)}, u32[]{:S(2)}) collective-permute-start(bf16[96,2048]{1,0:T(8,128)(2,1)S(1)} %get-tuple-element.54.refs_0_), channel_id=1, source_target_pairs={{0,1},{1,2},{2,3},{3,0},{4,5},{5,6},{6,7},{7,4},{8,9},{9,10},{10,1... | collective-permute-start | bytes 1179656 | tf_op jit(solution)/shard_map/ppermute | solution.py:633
  73.1 20.5 %collective-permute-start.11 = (bf16[96,2048]{1,0:T(8,128)(2,1)S(1)}, bf16[96,2048]{1,0:T(8,128)(2,1)S(1)}, u32[]{:S(2)}, u32[]{:S(2)}) collective-permute-start(bf16[96,2048]{1,0:T(8,128)(2,1)S(1)} %get-tuple-element.54.refs_0_), channel_id=1, source_target_pairs={{0,2},{1,3},{2,0},{3,1},{4,6},{5,7},{6,4},{7,5},{8,10},{9,11},{10,... | collective-permute-start | bytes 1179656 | tf_op jit(solution)/shard_map/ppermute | solution.py:632
  102.5 6.5 %collective-permute-start.15 = (bf16[48,2048]{1,0:T(8,128)(2,1)S(1)}, bf16[48,2048]{1,0:T(8,128)(2,1)S(1)}, u32[]{:S(2)}, u32[]{:S(2)}) collective-permute-start(bf16[48,2048]{1,0:T(8,128)(2,1)S(1)} %get-tuple-element.61), channel_id=1, source_target_pairs={{0,3},{1,0},{2,1},{3,2},{4,7},{5,4},{6,5},{7,6},{8,11},{9,8},{10,9... | collective-permute-start | bytes 589832 | tf_op jit(solution)/shard_map/ppermute | solution.py:637
  102.9 7.0 %collective-permute-start.16 = (bf16[48,2048]{1,0:T(8,128)(2,1)S(1)}, bf16[48,2048]{1,0:T(8,128)(2,1)S(1)}, u32[]{:S(2)}, u32[]{:S(2)}) collective-permute-start(bf16[48,2048]{1,0:T(8,128)(2,1)S(1)} %get-tuple-element.63), channel_id=1, source_target_pairs={{0,1},{1,2},{2,3},{3,0},{4,5},{5,6},{6,7},{7,4},{8,9},{9,10},{10,1... | collective-permute-start | bytes 589832 | tf_op jit(solution)/shard_map/ppermute | solution.py:636
  106.7 10.6 %collective-permute-start.14 = (bf16[48,2048]{1,0:T(8,128)(2,1)S(1)}, bf16[48,2048]{1,0:T(8,128)(2,1)S(1)}, u32[]{:S(2)}, u32[]{:S(2)}) collective-permute-start(bf16[48,2048]{1,0:T(8,128)(2,1)S(1)} %get-tuple-element.59), channel_id=1, source_target_pairs={{0,3},{1,0},{2,1},{3,2},{4,7},{5,4},{6,5},{7,6},{8,11},{9,8},{10,9... | collective-permute-start | bytes 589832 | tf_op jit(solution)/shard_map/ppermute | solution.py:639
  108.3 9.0 %collective-permute-start.19 = (bf16[48,2048]{1,0:T(8,128)(2,1)S(1)}, bf16[48,2048]{1,0:T(8,128)(2,1)S(1)}, u32[]{:S(2)}, u32[]{:S(2)}) collective-permute-start(bf16[48,2048]{1,0:T(8,128)(2,1)S(1)} %get-tuple-element.66), channel_id=1, source_target_pairs={{0,1},{1,2},{2,3},{3,0},{4,5},{5,6},{6,7},{7,4},{8,9},{9,10},{10,1... | collective-permute-start | bytes 589832 | tf_op jit(solution)/shard_map/ppermute | solution.py:640
  110.0 8.9 %collective-permute-start.17 = (bf16[48,2048]{1,0:T(8,128)(2,1)S(1)}, bf16[48,2048]{1,0:T(8,128)(2,1)S(1)}, u32[]{:S(2)}, u32[]{:S(2)}) collective-permute-start(bf16[48,2048]{1,0:T(8,128)(2,1)S(1)} %get-tuple-element.64), channel_id=1, source_target_pairs={{0,1},{1,2},{2,3},{3,0},{4,5},{5,6},{6,7},{7,4},{8,9},{9,10},{10,1... | collective-permute-start | bytes 589832 | tf_op jit(solution)/shard_map/ppermute | solution.py:643
  111.2 7.7 %collective-permute-start.18 = (bf16[48,2048]{1,0:T(8,128)(2,1)S(1)}, bf16[48,2048]{1,0:T(8,128)(2,1)S(1)}, u32[]{:S(2)}, u32[]{:S(2)}) collective-permute-start(bf16[48,2048]{1,0:T(8,128)(2,1)S(1)} %get-tuple-element.65), channel_id=1, source_target_pairs={{0,3},{1,0},{2,1},{3,2},{4,7},{5,4},{6,5},{7,6},{8,11},{9,8},{10,9... | collective-permute-start | bytes 589832 | tf_op jit(solution)/shard_map/ppermute | solution.py:642
Sparse Core Ops, SparseCore 0:
  9.6 79.5 all-gather.1
